TPU v7x, 32 devices: a whole 2x2x4 slice. The times are simulated.
32 devices in a mesh: ep: 16 (over z, y, x), tp: 2 (over core).
Axes of the slice: x: 2, y: 2, z: 4, core: 2. Of those that a mesh axis runs over, the one named last changes fastest.
Arguments:
- tokens: bfloat16 [128, 2048], P('ep'), may hold values from -6 to 6
- mixer_norm_gain: float32 [2048], replicated, may hold values from 0.1 to 1.9
- gate_projection_weight: bfloat16 [2048, 2, 2048], P(None, 'tp', 'ep'), may hold values from -0.125 to 0.125
- value_projection_weight: bfloat16 [2048, 2, 2048], P(None, 'tp', 'ep'), may hold values from -0.125 to 0.125
- input_projection_weight: bfloat16 [2048, 1024], P(None, 'tp'), may hold values from -0.125 to 0.125
- output_projection_weight: bfloat16 [2048, 1024], P(None, 'tp'), may hold values from -0.125 to 0.125
- step_projection_weight: bfloat16 [2048, 64], P(None, 'tp'), may hold values from -0.125 to 0.125
- head_step_bias: float32 [64], P('tp'), may hold values from -1 to 1
- head_decay_rate: float32 [64], P('tp'), may hold values from 0.02 to 3
- extra_log_decay: float32 [128, 64], P('ep', 'tp'), may hold values from -0.7 to 0
- value_taps: float32 [4, 4096], P(None, 'tp'), may hold values from -3 to 3
- input_taps: float32 [4, 1024], P(None, 'tp'), may hold values from -3 to 3
- output_taps: float32 [4, 1024], P(None, 'tp'), may hold values from -3 to 3
- prior_values: bfloat16 [128, 3, 4096], P('ep', None, 'tp'), may hold values from -6 to 6
- prior_input_maps: bfloat16 [128, 3, 1024], P('ep', None, 'tp'), may hold values from -6 to 6
- prior_output_maps: bfloat16 [128, 3, 1024], P('ep', None, 'tp'), may hold values from -6 to 6
- head_skip_gain: float32 [64], P('tp'), may hold values from 0.5 to 1.5
- group_norm_gain: float32 [4096], P('tp'), may hold values from 0.1 to 1.9
- mixer_output_weight: bfloat16 [4096, 2048], P('tp', 'ep'), may hold values from -0.09375 to 0.09375
- recurrent_state: float32 [128, 64, 64, 128], P('ep', 'tp'), may hold values from -6 to 6
- expert_norm_gain: float32 [2048], replicated, may hold values from 0.1 to 1.9
- routes: int32 [128, 6], P('ep'), may hold values from 0 to 15, all different within a row; in each aligned block of 8 rows (0 to 7, 8 to 15, ...) at most 4 rows name the same one
- chosen_expert_weight: float32 [128, 6], P('ep'), may hold values from 0.2 to 1
- routed_gate_weight: bfloat16 [16, 2048, 512], P('ep', None, 'tp'), may hold values from -0.125 to 0.125
- routed_up_weight: bfloat16 [16, 2048, 512], P('ep', None, 'tp'), may hold values from -0.125 to 0.125
- routed_down_weight: bfloat16 [16, 512, 2048], P('ep', 'tp'), may hold values from -0.25 to 0.25
- common_gate_weight: bfloat16 [2048, 512], P(None, 'tp'), may hold values from -0.125 to 0.125
- common_up_weight: bfloat16 [2048, 512], P(None, 'tp'), may hold values from -0.125 to 0.125
- common_down_weight: bfloat16 [512, 2048], P('tp'), may hold values from -0.25 to 0.25
Outputs:
- result: bfloat16 [128, 2048], P('ep')
- state_next: float32 [128, 64, 64, 128], P('ep', 'tp')
- next_value: bfloat16 [128, 3, 4096], P('ep', None, 'tp')
- next_input: bfloat16 [128, 3, 1024], P('ep', None, 'tp')
- next_output: bfloat16 [128, 3, 1024], P('ep', None, 'tp')
Inputs may be any that keep to these rules, and one draw needn't show every extreme that they name: `routes`: the 6 experts of a row differ; among the rows of one device (aligned blocks of 8 rows) no expert is named more than 4 times.
All inputs are finite; a program needn't handle non-finite values.
Results may differ from a plain program's by a relative error of at most 0.015.
Values may be sent and summed in bfloat16 or wider, within the bound.
A program may use at most 128 MiB of HBM per device.

v0:
```python
import functools

import jax
import jax.numpy as jnp
from jax import lax
from jax.experimental import pallas as pl
from jax.experimental.pallas import tpu as pltpu
from jax.sharding import PartitionSpec as P

D_INNER = 4096
GROUPS = 8


EPSILON = 1e-06


def rms_scale(values, gain_vec):
    values = values.astype(jnp.float32)
    return (
        values * lax.rsqrt(jnp.mean(values * values, axis=-1, keepdims=True) + EPSILON) * gain_vec
    )


def short_conv(past_rows, fresh_row, weight):
    window = jnp.concatenate([past_rows, fresh_row[:, None, :]], axis=1)
    summed = window[:, 0].astype(jnp.float32) * weight[0]
    for offset in range(1, window.shape[1]):
        summed = summed + window[:, offset].astype(jnp.float32) * weight[offset]
    return (jax.nn.silu(summed), window[:, 1:])


def state_step(
    state_prev, value_conv, input_conv, output_conv, timestep_size, step_decay, head_skip_gain
):
    batch_rows, head_count, head_size, state_size = state_prev.shape
    per_group = head_count // (input_conv.shape[1] // state_size)
    value_heads = value_conv.reshape(batch_rows, head_count, head_size)
    input_heads = jnp.repeat(input_conv.reshape(batch_rows, -1, state_size), per_group, axis=1)
    output_heads = jnp.repeat(output_conv.reshape(batch_rows, -1, state_size), per_group, axis=1)
    state_next = (
        step_decay[:, :, None, None] * state_prev
        + (timestep_size[:, :, None] * value_heads)[:, :, :, None] * input_heads[:, :, None, :]
    )
    mixed_heads = (
        jnp.sum(state_next * output_heads[:, :, None, :], axis=-1)
        + head_skip_gain[None, :, None] * value_heads
    )
    return (state_next, mixed_heads.reshape(batch_rows, -1))


def gated_norm(mixed_flat, gate_rows, group_norm_gain, group_width):
    gated_rows = mixed_flat * jax.nn.silu(gate_rows.astype(jnp.float32))
    grouped = gated_rows.reshape(gated_rows.shape[0], -1, group_width)
    grouped = grouped * lax.rsqrt(jnp.mean(grouped * grouped, axis=-1, keepdims=True) + EPSILON)
    return (grouped.reshape(gated_rows.shape[0], -1) * group_norm_gain).astype(jnp.bfloat16)


def expert_partial(arrived, gate_mat, up_mat, down_mat):
    gate_part = jnp.einsum("slcd,ldf->slcf", arrived, gate_mat, preferred_element_type=jnp.float32)
    up_part = jnp.einsum("slcd,ldf->slcf", arrived, up_mat, preferred_element_type=jnp.float32)
    hidden = (jax.nn.silu(gate_part) * up_part).astype(jnp.bfloat16)
    return jnp.einsum("slcf,lfd->slcd", hidden, down_mat, preferred_element_type=jnp.float32)


MESH = pl.DeviceIdType.MESH
BF16 = jnp.bfloat16
F32 = jnp.float32


def signal_all(n):
    me, t = lax.axis_index("ep"), lax.axis_index("tp")
    barrier = pltpu.get_barrier_semaphore()

    def tell(off, carry):
        p = lax.rem(me + off, n)
        pl.semaphore_signal(barrier, inc=1, device_id={"ep": p, "tp": t}, device_id_type=MESH)
        pl.semaphore_signal(barrier, inc=1, device_id={"ep": p, "tp": 1 - t}, device_id_type=MESH)
        return carry

    lax.fori_loop(1, n, tell, 0)
    pl.semaphore_signal(barrier, inc=1, device_id={"ep": me, "tp": 1 - t}, device_id_type=MESH)


def wait_all(n):
    pl.semaphore_wait(pltpu.get_barrier_semaphore(), 2 * n - 1)


def ep_send(n, source, target, send_sem, recv_sem):
    me, t = lax.axis_index("ep"), lax.axis_index("tp")

    def start(off, carry):
        p = lax.rem(me + off, n)
        pltpu.make_async_remote_copy(
            source(p), target(me), send_sem.at[off], recv_sem.at[me],
            device_id={"ep": p, "tp": t}, device_id_type=MESH,
        ).start()
        return carry

    lax.fori_loop(1, n, start, 0)


def ep_wait(n, target, send_sem, recv_sem, sends):
    me, t = lax.axis_index("ep"), lax.axis_index("tp")

    def finish(off, carry):
        p = lax.rem(me + n - off, n)
        copy = pltpu.make_async_remote_copy(
            target(p), target(p), send_sem.at[off], recv_sem.at[p],
            device_id={"ep": p, "tp": t}, device_id_type=MESH,
        )
        if sends:
            copy.wait_send()
        else:
            copy.wait_recv()
        return carry

    lax.fori_loop(1, n, finish, 0)


def partner_copy(source, target, send_sem, recv_sem):
    me, t = lax.axis_index("ep"), lax.axis_index("tp")
    return pltpu.make_async_remote_copy(
        source, target, send_sem, recv_sem,
        device_id={"ep": me, "tp": 1 - t}, device_id_type=MESH,
    )


def short_conv_in(past, fresh, taps, window):
    summed = past[0].astype(F32) * taps[0:1]
    for offset in range(1, past.shape[0]):
        summed = summed + past[offset].astype(F32) * taps[offset : offset + 1]
        window[offset - 1] = past[offset]
    window[past.shape[0] - 1] = fresh
    return jax.nn.silu(summed + fresh.astype(F32) * taps[past.shape[0] : past.shape[0] + 1])


def step_kernel(
    n, capacity,
    tokens, gain, step_bias, decay_rate, extra_decay, v_taps, i_taps, o_taps,
    v_past, i_past, o_past, skip, group_gain, gain2, routes, route_weight,
    state, gate_w, value_w, in_w, out_w, step_w, mix_w, cg_w, cu_w, cd_w, rg_w, ru_w, rd_w,
    result, state_out, v_next, i_next, o_next,
    mine, other, proj, back, held, old_mix, decays, columns,
    gath, part, got, out_blk, arr, ret, home, share, theirs,
    gw, vw, iw, ow, sw, wm, cg, cu, cd, rg, ru, rd,
    wsem, ssem, osem, gs, gr, ds0, dr0, rs, rr,
    as_, ar, ps, pr, xs, xr, ds, dr, es, er, fs, fr, hs, hr,
):
    me, t = lax.axis_index("ep"), lax.axis_index("tp")
    signal_all(n)
    rows, width = tokens.shape
    half = width // 2
    piece = gate_w.shape[1]
    groups, span, states = held.shape[1:]
    inner = groups * span
    heads = step_bias.shape[1]
    per_group = heads // groups
    head = span // per_group
    pairs = (
        (gate_w, gw), (value_w, vw), (in_w, iw), (out_w, ow), (step_w, sw), (mix_w, wm),
        (cg_w, cg), (cu_w, cu), (rg_w, rg), (ru_w, ru), (rd_w, rd), (cd_w, cd),
    )
    loads = [pltpu.make_async_copy(x, y, wsem.at[i]) for i, (x, y) in enumerate(pairs)]
    reads = [pltpu.make_async_copy(state.at[r], held.at[r], ssem.at[r]) for r in range(rows)]
    for load in loads[:5] + reads + loads[5:]:
        load.start()
    normed = rms_scale(tokens[...], gain[...]).astype(BF16)
    mine[me] = jnp.where(t == 0, normed[:, :half], normed[:, half:])
    wait_all(n)
    ep_send(n, lambda p: mine.at[me], lambda p: mine.at[p], gs, gr)

    for load in loads[:5]:
        load.wait()
    in_rows = jnp.dot(normed, iw[...], preferred_element_type=F32).astype(BF16)
    out_rows = jnp.dot(normed, ow[...], preferred_element_type=F32).astype(BF16)
    step_raw = jnp.dot(normed, sw[...], preferred_element_type=F32) + step_bias[...]
    in_conv = short_conv_in(i_past, in_rows, i_taps, i_next)
    out_conv = short_conv_in(o_past, out_rows, o_taps, o_next)
    step = jnp.maximum(step_raw, 0.0) + jnp.log1p(jnp.exp(-jnp.abs(step_raw)))
    decay = jnp.exp(-step * decay_rate[...] + extra_decay[...])
    decays[...] = decay
    own_head = lax.broadcasted_iota(jnp.int32, (heads, inner), 0)
    of_channel = lax.div(lax.broadcasted_iota(jnp.int32, (heads, inner), 1), head)
    spread_heads = jnp.where(own_head == of_channel, 1.0, 0.0).astype(F32)
    stacked = jnp.concatenate(
        [step, decay, jnp.broadcast_to(skip[...], (rows, heads))], axis=0
    )
    wide = jnp.dot(
        stacked, spread_heads, precision=lax.Precision.HIGHEST, preferred_element_type=F32
    )
    step_wide, decay_wide, skip_wide = wide[:rows], wide[rows : 2 * rows], wide[2 * rows :]

    lane = lax.broadcasted_iota(jnp.int32, (rows, n * rows), 1)
    lane_expert, lane_slot = lax.div(lane, rows), lax.rem(lane, capacity)
    named = jnp.zeros((rows, n * rows), F32)
    weighted = jnp.zeros((rows, n * rows), F32)
    for k in range(routes.shape[1]):
        hit = routes[:, k : k + 1] == lane_expert
        named = named + jnp.where(hit, 1.0, 0.0)
        weighted = weighted + jnp.where(hit, route_weight[:, k : k + 1], 0.0)
    row_id = lax.broadcasted_iota(jnp.int32, (rows, n * rows), 0)
    earlier = jnp.zeros((rows, n * rows), F32)
    for r in range(rows - 1):
        earlier = earlier + jnp.where(row_id > r, named[r : r + 1], 0.0)
    filled = jnp.where(earlier == lane_slot.astype(F32), named, 0.0)
    spread = jnp.transpose(filled).astype(BF16)
    low_lane = lax.rem(lane, rows) < capacity
    weighted = weighted * filled
    combine = jnp.concatenate(
        [jnp.where(low_lane, weighted, 0.0), jnp.where(low_lane, 0.0, weighted)], axis=0
    )

    ep_wait(n, lambda p: mine.at[p], gs, gr, False)
    cross = partner_copy(mine, other, ds0, dr0)
    cross.start()

    def product(block_ref, start):
        block = block_ref[...].reshape(n * rows, half)
        return [
            jnp.dot(block, w[pl.ds(start, half)], preferred_element_type=F32) for w in (gw, vw)
        ]

    first = product(mine, pl.multiple_of(t * half, half))
    cross.wait_recv()
    second = product(other, pl.multiple_of((1 - t) * half, half))
    for k in range(2):
        proj[:, k] = (first[k] + second[k]).astype(BF16).reshape(n, rows, piece)
    back[me] = proj[me]
    ep_send(n, lambda p: proj.at[p], lambda p: back.at[p], rs, rr)

    for read in reads:
        read.wait()
    span_row = lax.broadcasted_iota(jnp.int32, (rows, span), 0)
    for g in range(groups):
        maps = out_conv[:, g * states : (g + 1) * states].astype(BF16)

        def reduce_row(r, acc, g=g, maps=maps):
            block = held[r, g].astype(BF16)
            sums = lax.dot_general(
                maps, block, (((1,), (1,)), ((), ())), preferred_element_type=F32
            )
            return jnp.where(span_row == r, sums, acc)

        old_mix[:, g * span : (g + 1) * span] = lax.fori_loop(
            0, rows, reduce_row, jnp.zeros((rows, span), F32)
        )

    ep_wait(n, lambda p: back.at[p], rs, rr, False)
    gate_rows = jnp.concatenate([back[j, 0] for j in range(n)], axis=1).astype(F32)
    value_rows = jnp.concatenate([back[j, 1] for j in range(n)], axis=1)
    value_conv = short_conv_in(v_past, value_rows, v_taps, v_next)
    scaled = step_wide * value_conv
    gate = jax.nn.silu(gate_rows)
    for g in range(groups):
        cut, maps = slice(g * span, (g + 1) * span), slice(g * states, (g + 1) * states)
        overlap = jnp.sum(in_conv[:, maps] * out_conv[:, maps], axis=-1, keepdims=True)
        mix = (
            decay_wide[:, cut] * old_mix[:, cut]
            + scaled[:, cut] * overlap
            + skip_wide[:, cut] * value_conv[:, cut]
        ) * gate[:, cut]
        mix = mix * lax.rsqrt(jnp.mean(mix * mix, axis=-1, keepdims=True) + EPSILON)
        gath[me, :, cut] = (mix * group_gain[:, cut]).astype(BF16)
    ep_send(n, lambda p: gath.at[me], lambda p: gath.at[p], as_, ar)

    top = scaled.astype(BF16).astype(F32)
    rest = scaled - top
    columns[...] = jnp.transpose(jnp.concatenate([top, rest, top], axis=0)).astype(BF16)
    map_row = lax.rem(lax.broadcasted_iota(jnp.int32, (3 * rows, states), 0), rows)

    def state_store(r):
        return pltpu.make_async_copy(held.at[r], state_out.at[r], osem.at[r])

    def update_row(r, carry):
        decay_row = decays[pl.ds(r, 1), :]
        for g in range(groups):
            maps = in_conv[:, g * states : (g + 1) * states]
            high = maps.astype(BF16).astype(F32)
            triple = jnp.concatenate([high, high, maps - high], axis=0)
            picked = jnp.where(map_row == r, triple, 0.0).astype(BF16)
            grown = jnp.dot(
                columns[g * span : (g + 1) * span, :], picked, preferred_element_type=F32
            )
            for h in range(per_group):
                at = slice(h * head, (h + 1) * head)
                factor = decay_row[:, g * per_group + h : g * per_group + h + 1]
                held[r, g, at, :] = held[r, g, at, :] * factor + grown[at]
        state_store(r).start()
        return carry

    lax.fori_loop(0, rows, update_row, 0)
    for load in loads[5:]:
        load.wait()
    ep_wait(n, lambda p: gath.at[p], as_, ar, False)
    summed = jnp.dot(
        gath[...].reshape(n * rows, inner), wm[...], preferred_element_type=F32
    )
    part[...] = summed.astype(BF16).reshape(n, rows, piece)
    got[t, me] = part[me]

    def start(off, carry):
        p = lax.rem(me + off, n)
        pltpu.make_async_remote_copy(
            part.at[p], got.at[t, me], ps.at[off], pr.at[me],
            device_id={"ep": p, "tp": t}, device_id_type=MESH,
        ).start()
        pltpu.make_async_remote_copy(
            part.at[p], got.at[t, me], xs.at[off], xr.at[me],
            device_id={"ep": p, "tp": 1 - t}, device_id_type=MESH,
        ).start()
        return carry

    lax.fori_loop(1, n, start, 0)
    near = partner_copy(part.at[me], got.at[t, me], ds, dr)
    near.start()
    near_in = partner_copy(part.at[me], got.at[1 - t, me], ds, dr)
    near_in.wait_recv()
    ep_wait(n, lambda p: got.at[t, p], ps, pr, False)
    ep_wait(n, lambda p: got.at[1 - t, p], xs, xr, False)
    both = (got[0].astype(F32) + got[1].astype(F32)).astype(BF16).astype(F32)
    mixed_out = jnp.concatenate([both[j] for j in range(n)], axis=1)
    stream = (tokens[...].astype(F32) + mixed_out).astype(BF16)
    ffn = rms_scale(stream, gain2[...]).astype(BF16)

    upper = lax.rem(lax.broadcasted_iota(jnp.int32, (n * rows, 1), 0), rows) >= rows // 2
    left = jnp.dot(spread, ffn[:, :half], preferred_element_type=F32)
    right = jnp.dot(spread, ffn[:, half:], preferred_element_type=F32)
    out_blk[...] = jnp.where(upper, right, left).astype(BF16).reshape(n, rows, half)
    arr[me] = out_blk[me]
    ep_send(n, lambda p: out_blk.at[p], lambda p: arr.at[p], es, er)
    shared_hidden = (
        jax.nn.silu(jnp.dot(ffn, cg[...], preferred_element_type=F32))
        * jnp.dot(ffn, cu[...], preferred_element_type=F32)
    ).astype(BF16)
    shared = jnp.dot(shared_hidden, cd[...], preferred_element_type=F32)
    ep_wait(n, lambda p: arr.at[p], es, er, False)

    arrived = arr[...].reshape(n * rows, half)

    def up(w):
        low = jnp.dot(arrived, w[:half], preferred_element_type=F32)
        high = jnp.dot(arrived, w[half:], preferred_element_type=F32)
        count = n * rows
        other = jnp.where(
            upper, pltpu.roll(low, rows // 2, 0), pltpu.roll(high, count - rows // 2, 0)
        )
        return jnp.where(upper, high, low) + other

    hidden = (jax.nn.silu(up(rg)) * up(ru)).astype(BF16)
    out_left = jnp.dot(hidden, rd[:, :half], preferred_element_type=F32)
    out_right = jnp.dot(hidden, rd[:, half:], preferred_element_type=F32)
    ret[...] = jnp.where(upper, out_right, out_left).astype(BF16).reshape(n, rows, half)
    home[me] = ret[me]
    ep_send(n, lambda p: ret.at[p], lambda p: home.at[p], fs, fr)
    ep_wait(n, lambda p: home.at[p], fs, fr, False)
    routed = jnp.dot(
        combine, home[...].reshape(n * rows, half).astype(F32),
        precision=lax.Precision.HIGHEST, preferred_element_type=F32,
    )
    share[:, :half] = shared[:, :half] + routed[:rows]
    share[:, half:] = shared[:, half:] + routed[rows:]
    last = partner_copy(share, theirs, hs, hr)
    last.start()
    last.wait_recv()
    result[...] = (stream.astype(F32) + (share[...] + theirs[...])).astype(BF16)
    ep_wait(n, lambda p: gath.at[p], as_, ar, True)
    ep_wait(n, lambda p: got.at[t, p], ps, pr, True)
    ep_wait(n, lambda p: got.at[t, p], xs, xr, True)
    near.wait_send()
    ep_wait(n, lambda p: arr.at[p], es, er, True)
    ep_wait(n, lambda p: home.at[p], fs, fr, True)
    last.wait_send()
    ep_wait(n, lambda p: mine.at[p], gs, gr, True)
    cross.wait_send()
    ep_wait(n, lambda p: back.at[p], rs, rr, True)
    for row in range(rows):
        state_store(row).wait()


def mixer_step(n, capacity, small, state, weights):
    rows, width = small[0].shape
    half = width // 2
    piece = weights[0].shape[1]
    inner = n * piece
    groups, span, _ = state.shape[1:]
    vmem, hbm = pl.BlockSpec(memory_space=pltpu.VMEM), pl.BlockSpec(memory_space=pl.ANY)
    dma = pltpu.SemaphoreType.DMA
    many = dma((n,))
    block = pltpu.VMEM((n, rows, half), BF16)
    pieces = pltpu.VMEM((n, 2, rows, piece), BF16)
    heads = small[2].shape[1]
    shape = jax.ShapeDtypeStruct
    mix_piece = weights[5].shape[1]
    return pl.pallas_call(
        functools.partial(step_kernel, n, capacity),
        out_shape=(
            shape((rows, width), BF16),
            shape(state.shape, F32),
            shape(small[8].shape, BF16),
            shape(small[9].shape, BF16),
            shape(small[10].shape, BF16),
        ),
        in_specs=[vmem] * len(small) + [hbm] * (1 + len(weights)),
        out_specs=(vmem, hbm, vmem, vmem, vmem),
        scratch_shapes=[
            block, block, pieces, pieces,
            pltpu.VMEM(state.shape, F32),
            pltpu.VMEM((rows, inner), F32),
            pltpu.VMEM((rows, heads), F32),
            pltpu.VMEM((inner, 3 * rows), BF16),
            pltpu.VMEM((n, rows, inner), BF16),
            pltpu.VMEM((n, rows, mix_piece), BF16),
            pltpu.VMEM((2, n, rows, mix_piece), BF16),
            block, block, block, block,
            pltpu.VMEM((rows, width), F32),
            pltpu.VMEM((rows, width), F32),
        ]
        + [pltpu.VMEM(w.shape, BF16) for w in weights[:9]]
        + [pltpu.VMEM(w.shape, BF16) for w in weights[9:]]
        + [dma((12,)), dma((rows,)), dma((rows,)), many, many, dma, dma, many, many]
        + [many] * 6 + [dma, dma] + [many] * 4 + [dma, dma],
        compiler_params=pltpu.CompilerParams(collective_id=0, has_side_effects=True),
    )(*small, state, *weights)


def fast_shards(
    tokens,
    mixer_norm_gain,
    gate_projection_weight,
    value_projection_weight,
    input_projection_weight,
    output_projection_weight,
    step_projection_weight,
    head_step_bias,
    head_decay_rate,
    extra_log_decay,
    value_taps,
    input_taps,
    output_taps,
    prior_values,
    prior_input_maps,
    prior_output_maps,
    head_skip_gain,
    group_norm_gain,
    mixer_output_weight,
    recurrent_state,
    expert_norm_gain,
    routes,
    chosen_expert_weight,
    routed_gate_weight,
    routed_up_weight,
    routed_down_weight,
    common_gate_weight,
    common_up_weight,
    common_down_weight,
):
    seq_rows, model_width = tokens.shape
    ep_count = lax.axis_size("ep")
    capacity = (seq_rows * routes.shape[1] + ep_count - 1) // ep_count + 1

    def one_row(vector):
        return vector.reshape(1, -1)

    def flat(weight):
        return weight.reshape(model_width, -1)

    states = recurrent_state.shape[3]
    group_count = input_projection_weight.shape[1] // states
    small = (
        tokens, one_row(mixer_norm_gain), one_row(head_step_bias), one_row(head_decay_rate),
        extra_log_decay, value_taps, input_taps, output_taps,
        prior_values.transpose(1, 0, 2), prior_input_maps.transpose(1, 0, 2),
        prior_output_maps.transpose(1, 0, 2), one_row(head_skip_gain), one_row(group_norm_gain),
        one_row(expert_norm_gain), routes, chosen_expert_weight,
    )
    weights = (
        flat(gate_projection_weight), flat(value_projection_weight), input_projection_weight,
        output_projection_weight, step_projection_weight, mixer_output_weight,
        common_gate_weight, common_up_weight, common_down_weight,
        routed_gate_weight.reshape(routed_gate_weight.shape[1:]),
        routed_up_weight.reshape(routed_up_weight.shape[1:]),
        routed_down_weight.reshape(routed_down_weight.shape[1:]),
    )
    result, state_next, next_value, next_input, next_output = mixer_step(
        ep_count, capacity, small,
        recurrent_state.reshape(seq_rows, group_count, -1, states), weights,
    )
    return (
        result,
        state_next.reshape(recurrent_state.shape),
        next_value.transpose(1, 0, 2),
        next_input.transpose(1, 0, 2),
        next_output.transpose(1, 0, 2),
    )


def fits_kernels(rows, n, tp, gate_w, mix_w, routes, routed_w):
    if tp != 2 or routed_w.shape[0] != 1 or rows != 8:
        return False
    capacity = (rows * routes.shape[1] + n - 1) // n + 1
    return gate_w.shape[2] % 128 == 0 and mix_w.shape[1] % 128 == 0 and 2 * capacity == rows


def shards(
    tokens,
    mixer_norm_gain,
    gate_projection_weight,
    value_projection_weight,
    input_projection_weight,
    output_projection_weight,
    step_projection_weight,
    head_step_bias,
    head_decay_rate,
    extra_log_decay,
    value_taps,
    input_taps,
    output_taps,
    prior_values,
    prior_input_maps,
    prior_output_maps,
    head_skip_gain,
    group_norm_gain,
    mixer_output_weight,
    recurrent_state,
    expert_norm_gain,
    routes,
    chosen_expert_weight,
    routed_gate_weight,
    routed_up_weight,
    routed_down_weight,
    common_gate_weight,
    common_up_weight,
    common_down_weight,
):
    seq_rows, model_width = tokens.shape
    ep_count = lax.axis_size("ep")
    tp_count = lax.axis_size("tp")
    if fits_kernels(seq_rows, ep_count, tp_count, gate_projection_weight, mixer_output_weight, routes, routed_gate_weight):
        return fast_shards(
            tokens, mixer_norm_gain, gate_projection_weight, value_projection_weight,
            input_projection_weight, output_projection_weight, step_projection_weight,
            head_step_bias, head_decay_rate, extra_log_decay, value_taps, input_taps,
            output_taps, prior_values, prior_input_maps, prior_output_maps, head_skip_gain,
            group_norm_gain, mixer_output_weight, recurrent_state, expert_norm_gain, routes,
            chosen_expert_weight, routed_gate_weight, routed_up_weight, routed_down_weight,
            common_gate_weight, common_up_weight, common_down_weight,
        )
    tp_place = lax.axis_index("tp")
    normed = rms_scale(tokens, mixer_norm_gain).astype(jnp.bfloat16)
    both_pieces = jnp.concatenate(
        [
            gate_projection_weight.reshape(model_width, -1),
            value_projection_weight.reshape(model_width, -1),
        ],
        axis=1,
    )
    piece_width = both_pieces.shape[1] // 2
    projected = jnp.dot(
        lax.all_gather(normed, "ep", axis=0, tiled=True),
        both_pieces,
        preferred_element_type=jnp.float32,
    ).astype(jnp.bfloat16)
    returned = lax.all_to_all(projected, "ep", split_axis=0, concat_axis=1, tiled=True).reshape(
        seq_rows, ep_count, 2, piece_width
    )
    gate_rows = returned[:, :, 0].reshape(seq_rows, -1)
    value_rows = returned[:, :, 1].reshape(seq_rows, -1)
    input_rows = jnp.dot(
        normed, input_projection_weight, preferred_element_type=jnp.float32
    ).astype(jnp.bfloat16)
    output_rows = jnp.dot(
        normed, output_projection_weight, preferred_element_type=jnp.float32
    ).astype(jnp.bfloat16)
    step_raw = jnp.dot(normed, step_projection_weight, preferred_element_type=jnp.float32)
    value_conv, next_value = short_conv(prior_values, value_rows, value_taps)
    input_conv, next_input = short_conv(prior_input_maps, input_rows, input_taps)
    output_conv, next_output = short_conv(prior_output_maps, output_rows, output_taps)
    timestep_size = jax.nn.softplus(step_raw + head_step_bias)
    step_decay = jnp.exp(-timestep_size * head_decay_rate + extra_log_decay)
    state_next, mixed_flat = state_step(
        recurrent_state,
        value_conv,
        input_conv,
        output_conv,
        timestep_size,
        step_decay,
        head_skip_gain,
    )
    mixer_rows = gated_norm(mixed_flat, gate_rows, group_norm_gain, D_INNER // GROUPS)
    partial_mix = jnp.dot(
        lax.all_gather(mixer_rows, "ep", axis=0, tiled=True),
        mixer_output_weight,
        preferred_element_type=jnp.float32,
    )
    mix_share = lax.psum_scatter(
        partial_mix.reshape(ep_count, seq_rows, -1).astype(jnp.bfloat16),
        "tp",
        scatter_dimension=1,
        tiled=True,
    )
    moved_mix = lax.all_to_all(mix_share, "ep", split_axis=0, concat_axis=2, tiled=True)
    mixed_out = lax.all_gather(moved_mix, "tp", axis=1, tiled=True).reshape(seq_rows, model_width)
    stream = (tokens.astype(jnp.float32) + mixed_out.astype(jnp.float32)).astype(jnp.bfloat16)
    ffn_rows = rms_scale(stream, expert_norm_gain).astype(jnp.bfloat16)
    shared_hidden = (
        jax.nn.silu(jnp.dot(ffn_rows, common_gate_weight, preferred_element_type=jnp.float32))
        * jnp.dot(ffn_rows, common_up_weight, preferred_element_type=jnp.float32)
    ).astype(jnp.bfloat16)
    shared_out = lax.psum(
        jnp.dot(shared_hidden, common_down_weight, preferred_element_type=jnp.float32).astype(
            jnp.bfloat16
        ),
        "tp",
    ).astype(jnp.float32)
    exp_local = routed_gate_weight.shape[0]
    expert_total = exp_local * ep_count
    topk_count = routes.shape[1]
    capacity = (seq_rows * topk_count + expert_total - 1) // expert_total + 1
    slot_count = expert_total * capacity
    expert_ids = jnp.arange(expert_total, dtype=jnp.int32)
    flat_routes = routes.reshape(-1)
    onehot = (flat_routes[:, None] == expert_ids[None, :]).astype(jnp.int32)
    slot_ids = jnp.sum((jnp.cumsum(onehot, axis=0) - onehot) * onehot, axis=1)
    positions = flat_routes * capacity + slot_ids
    matches = (jnp.arange(slot_count, dtype=jnp.int32)[:, None] == positions[None, :]).reshape(
        slot_count, seq_rows, topk_count
    )
    dispatch_mat = jnp.sum(matches.astype(jnp.float32), axis=2).astype(jnp.bfloat16)
    combine_mat = jnp.sum(jnp.where(matches, chosen_expert_weight[None], 0.0), axis=2)
    outgoing = jnp.dot(dispatch_mat, ffn_rows, preferred_element_type=jnp.float32).astype(
        jnp.bfloat16
    )
    outgoing = outgoing.reshape(ep_count, exp_local, capacity, model_width)
    half_width = model_width // tp_count
    own_cols = lax.dynamic_slice_in_dim(outgoing, tp_place * half_width, half_width, 3)
    full_rows = lax.all_gather(
        lax.all_to_all(own_cols, "ep", split_axis=0, concat_axis=0, tiled=True),
        "tp",
        axis=3,
        tiled=True,
    )
    partial_out = expert_partial(
        full_rows, routed_gate_weight, routed_up_weight, routed_down_weight
    )
    share_out = lax.psum_scatter(
        partial_out.astype(jnp.bfloat16), "tp", scatter_dimension=3, tiled=True
    )
    back_half = lax.all_to_all(share_out, "ep", split_axis=0, concat_axis=0, tiled=True)
    routed_half = lax.dot_general(
        combine_mat,
        back_half.reshape(slot_count, half_width).astype(jnp.float32),
        (((0,), (0,)), ((), ())),
        precision=lax.Precision.HIGHEST,
    )
    routed = lax.all_gather(routed_half.astype(jnp.bfloat16), "tp", axis=1, tiled=True).astype(
        routed_half.dtype
    )
    result = (stream.astype(jnp.float32) + shared_out + routed).astype(jnp.bfloat16)
    return (result, state_next, next_value, next_input, next_output)


def solution(mesh):
    return jax.shard_map(
        shards,
        mesh=mesh,
        in_specs=(
            P("ep", None),
            P(),
            P(None, "tp", "ep"),
            P(None, "tp", "ep"),
            P(None, "tp"),
            P(None, "tp"),
            P(None, "tp"),
            P("tp"),
            P("tp"),
            P("ep", "tp"),
            P(None, "tp"),
            P(None, "tp"),
            P(None, "tp"),
            P("ep", None, "tp"),
            P("ep", None, "tp"),
            P("ep", None, "tp"),
            P("tp"),
            P("tp"),
            P("tp", "ep"),
            P("ep", "tp", None, None),
            P(),
            P("ep", None),
            P("ep", None),
            P("ep", None, "tp"),
            P("ep", None, "tp"),
            P("ep", "tp", None),
            P(None, "tp"),
            P(None, "tp"),
            P("tp", None),
        ),
        out_specs=(
            P("ep", None),
            P("ep", "tp", None, None),
            P("ep", None, "tp"),
            P("ep", None, "tp"),
            P("ep", None, "tp"),
        ),
        check_vma=False,
    )
```

profile of v0, /device:TPU:0, one launch (start us, length us, event | category | flops | bytes accessed | tf_op | source)
XLA Modules:
  0.0 75.4 jit_solution(7197491379478534693)
XLA Ops:
  0.6 1.9 %copy.34.step_w = bf16[2048,32]{1,0:T(8,128)(2,1)} copy(bf16[2048,32]{0,1:T(8,128)(2,1)} %param.35) | data formatting | bytes 262144 | tf_op args[6]
  2.5 61.2 %shard_map.308 = (bf16[8,2048]{1,0:T(8,128)(2,1)}, f32[8,4,512,128]{3,2,1,0:T(8,128)}, bf16[3,8,2048]{2,1,0:T(8,128)(2,1)}, bf16[3,8,512]{2,1,0:T(8,128)(2,1)}, bf16[3,8,512]{2,1,0:T(8,128)(2,1)}) custom-call(bf16[8,2048]{1,0:T(8,128)(2,1)} %tokens.1, f32[1,2048]{1,0:T(1,128)} %bitcast.32, f32[1,32]{1,0:T(1,128)} %bitcast.35, f32[1,32]{1,0:T(1,128)} %bitcast.36, ...), custom_call_target="tpu_custom_call" | custom-call | tf_op jit(solution)/shard_map/pallas_call | solution.py:394
  63.7 1.4 %copy.40 = bf16[8,2048]{1,0:T(8,128)(2,1)} copy(bf16[8,2048]{1,0:T(8,128)(2,1)} %get-tuple-element.20) | data formatting | bytes 65536
  65.1 0.0 copy-start
  65.1 0.0 copy-start.2
  65.1 0.0 copy-start.1
  65.1 8.5 %copy.41 = f32[8,32,64,128]{3,2,1,0:T(8,128)} copy(f32[8,32,64,128]{3,2,1,0:T(8,128)} %bitcast.19) | data formatting | bytes 16777216
  73.6 0.0 copy-done
  73.6 0.6 copy.42
  74.2 0.0 copy-done.2
  74.2 0.6 copy.43
  74.8 0.0 copy-done.1
  74.8 0.6 copy.44
Async XLA Ops:
  65.1 8.5 %copy-start = (bf16[3,8,2048]{2,1,0:T(8,128)(2,1)S(1)}, bf16[3,8,2048]{2,1,0:T(8,128)(2,1)}, u32[]{:S(2)}) copy-start(bf16[3,8,2048]{2,1,0:T(8,128)(2,1)} %get-tuple-element.12) | copy-start | bytes 294916
  65.1 9.1 %copy-start.2 = (bf16[3,8,512]{2,1,0:T(8,128)(2,1)S(1)}, bf16[3,8,512]{2,1,0:T(8,128)(2,1)}, u32[]{:S(2)}) copy-start(bf16[3,8,512]{2,1,0:T(8,128)(2,1)} %get-tuple-element.13) | copy-start | bytes 73732
  65.1 9.7 %copy-start.1 = (bf16[3,8,512]{2,1,0:T(8,128)(2,1)S(1)}, bf16[3,8,512]{2,1,0:T(8,128)(2,1)}, u32[]{:S(2)}) copy-start(bf16[3,8,512]{2,1,0:T(8,128)(2,1)} %get-tuple-element.14) | copy-start | bytes 73732
where the time goes:
time: 76.1 us; the launch traced here: 75.4 us
  Pallas kernels  61.2 us (80%)
  local copies, waits for them, and re-layouts  13.6 us (18%)
    pallas_call x1, Pallas kernels, mixer_step(): pl.pallas_call(functools.partial(step_kernel, n, capacity), out_shape=(sh...  61.2 us
    unnamed x12, local copies, waits for them, and re-layouts  13.6 us

commit v1 on v0

--- a/solution.py
+++ b/solution.py
@@ -139,11 +139,11 @@
     tokens, gain, step_bias, decay_rate, extra_decay, v_taps, i_taps, o_taps,
     v_past, i_past, o_past, skip, group_gain, gain2, routes, route_weight,
     state, gate_w, value_w, in_w, out_w, step_w, mix_w, cg_w, cu_w, cd_w, rg_w, ru_w, rd_w,
-    result, state_out, v_next, i_next, o_next,
-    mine, other, proj, back, held, old_mix, decays, columns,
+    result, held, v_next, i_next, o_next,
+    mine, other, proj, back, old_mix, decays, columns,
     gath, part, got, out_blk, arr, ret, home, share, theirs,
     gw, vw, iw, ow, sw, wm, cg, cu, cd, rg, ru, rd,
-    wsem, ssem, osem, gs, gr, ds0, dr0, rs, rr,
+    wsem, ssem, gs, gr, ds0, dr0, rs, rr,
     as_, ar, ps, pr, xs, xr, ds, dr, es, er, fs, fr, hs, hr,
 ):
     me, t = lax.axis_index("ep"), lax.axis_index("tp")
@@ -173,7 +173,9 @@
         load.wait()
     in_rows = jnp.dot(normed, iw[...], preferred_element_type=F32).astype(BF16)
     out_rows = jnp.dot(normed, ow[...], preferred_element_type=F32).astype(BF16)
-    step_raw = jnp.dot(normed, sw[...], preferred_element_type=F32) + step_bias[...]
+    step_raw = lax.dot_general(
+        normed, sw[...], (((1,), (1,)), ((), ())), preferred_element_type=F32
+    ) + step_bias[...]
     in_conv = short_conv_in(i_past, in_rows, i_taps, i_next)
     out_conv = short_conv_in(o_past, out_rows, o_taps, o_next)
     step = jnp.maximum(step_raw, 0.0) + jnp.log1p(jnp.exp(-jnp.abs(step_raw)))
@@ -268,9 +270,6 @@
     columns[...] = jnp.transpose(jnp.concatenate([top, rest, top], axis=0)).astype(BF16)
     map_row = lax.rem(lax.broadcasted_iota(jnp.int32, (3 * rows, states), 0), rows)
 
-    def state_store(r):
-        return pltpu.make_async_copy(held.at[r], state_out.at[r], osem.at[r])
-
     def update_row(r, carry):
         decay_row = decays[pl.ds(r, 1), :]
         for g in range(groups):
@@ -285,7 +284,6 @@
                 at = slice(h * head, (h + 1) * head)
                 factor = decay_row[:, g * per_group + h : g * per_group + h + 1]
                 held[r, g, at, :] = held[r, g, at, :] * factor + grown[at]
-        state_store(r).start()
         return carry
 
     lax.fori_loop(0, rows, update_row, 0)
@@ -373,8 +371,6 @@
     ep_wait(n, lambda p: mine.at[p], gs, gr, True)
     cross.wait_send()
     ep_wait(n, lambda p: back.at[p], rs, rr, True)
-    for row in range(rows):
-        state_store(row).wait()
 
 
 def mixer_step(n, capacity, small, state, weights):
@@ -394,17 +390,16 @@
     return pl.pallas_call(
         functools.partial(step_kernel, n, capacity),
         out_shape=(
-            shape((rows, width), BF16),
-            shape(state.shape, F32),
-            shape(small[8].shape, BF16),
-            shape(small[9].shape, BF16),
-            shape(small[10].shape, BF16),
+            pltpu.VMEM((rows, width), BF16),
+            pltpu.VMEM(state.shape, F32),
+            pltpu.VMEM(small[8].shape, BF16),
+            pltpu.VMEM(small[9].shape, BF16),
+            pltpu.VMEM(small[10].shape, BF16),
         ),
         in_specs=[vmem] * len(small) + [hbm] * (1 + len(weights)),
-        out_specs=(vmem, hbm, vmem, vmem, vmem),
+        out_specs=(vmem,) * 5,
         scratch_shapes=[
             block, block, pieces, pieces,
-            pltpu.VMEM(state.shape, F32),
             pltpu.VMEM((rows, inner), F32),
             pltpu.VMEM((rows, heads), F32),
             pltpu.VMEM((inner, 3 * rows), BF16),
@@ -417,10 +412,38 @@
         ]
         + [pltpu.VMEM(w.shape, BF16) for w in weights[:9]]
         + [pltpu.VMEM(w.shape, BF16) for w in weights[9:]]
-        + [dma((12,)), dma((rows,)), dma((rows,)), many, many, dma, dma, many, many]
+        + [dma((12,)), dma((rows,)), many, many, dma, dma, many, many]
         + [many] * 6 + [dma, dma] + [many] * 4 + [dma, dma],
-        compiler_params=pltpu.CompilerParams(collective_id=0, has_side_effects=True),
+        compiler_params=pltpu.CompilerParams(
+            collective_id=0, has_side_effects=True, vmem_limit_bytes=54 << 20
+        ),
     )(*small, state, *weights)
+
+
+def store_kernel(count, *refs):
+    inputs, outputs, sems = refs[:count], refs[count : 2 * count], refs[2 * count]
+    rows = inputs[0].shape[0]
+    copies = [
+        pltpu.make_async_copy(inputs[0].at[r], outputs[0].at[r], sems.at[r]) for r in range(rows)
+    ]
+    for k in range(1, count):
+        copies.append(pltpu.make_async_copy(inputs[k], outputs[k], sems.at[rows + k - 1]))
+    for copy in copies:
+        copy.start()
+    for copy in copies:
+        copy.wait()
+
+
+def store(*arrays):
+    count = len(arrays)
+    return pl.pallas_call(
+        functools.partial(store_kernel, count),
+        out_shape=tuple(jax.ShapeDtypeStruct(a.shape, a.dtype) for a in arrays),
+        in_specs=[pl.BlockSpec(memory_space=pltpu.VMEM)] * count,
+        out_specs=(pl.BlockSpec(memory_space=pl.ANY),) * count,
+        scratch_shapes=[pltpu.SemaphoreType.DMA((arrays[0].shape[0] + count - 1,))],
+        compiler_params=pltpu.CompilerParams(vmem_limit_bytes=1 << 20),
+    )(*[pltpu.with_memory_space_constraint(a, pltpu.VMEM) for a in arrays])
 
 
 def fast_shards(
@@ -475,7 +498,7 @@
     )
     weights = (
         flat(gate_projection_weight), flat(value_projection_weight), input_projection_weight,
-        output_projection_weight, step_projection_weight, mixer_output_weight,
+        output_projection_weight, step_projection_weight.T, mixer_output_weight,
         common_gate_weight, common_up_weight, common_down_weight,
         routed_gate_weight.reshape(routed_gate_weight.shape[1:]),
         routed_up_weight.reshape(routed_up_weight.shape[1:]),
@@ -484,6 +507,9 @@
     result, state_next, next_value, next_input, next_output = mixer_step(
         ep_count, capacity, small,
         recurrent_state.reshape(seq_rows, group_count, -1, states), weights,
+    )
+    state_next, result, next_value, next_input, next_output = store(
+        state_next, result, next_value, next_input, next_output
     )
     return (
         result,

time: 76.1 us -> 65.1 us (0.86)
  local copies, waits for them, and re-layouts: 13.6 us -> 0 us
  Pallas kernels: 61.2 us -> 63.9 us
    unnamed x12 -> x0, local copies, waits for them, and re-layouts: 13.6 us -> none
    pallas_call x1 -> x2, Pallas kernels: 61.2 us -> 63.9 us  [the longest x1 60.5 us: mixer_step(): pl.pallas_call(functools.partial(step_kernel, n, capacity), out_shape=(pl...]
where the time goes in v1:
time: 65.1 us; the launch traced here: 64.5 us
  Pallas kernels  63.9 us (98%)
    pallas_call x1, Pallas kernels, mixer_step(): pl.pallas_call(functools.partial(step_kernel, n, capacity), out_shape=(pl...  60.5 us
    pallas_call x1, Pallas kernels, store(): pl.pallas_call(functools.partial(store_kernel, count), out_shape=tuple((j...  3.41 us

profile of v1, /device:TPU:0, one launch (start us, length us, event | category | flops | bytes accessed | tf_op | source)
XLA Modules:
  0.0 64.5 jit_solution(8723933212446967176)
XLA Ops:
  0.6 60.5 %shard_map.308 = (bf16[8,2048]{1,0:T(8,128)(2,1)S(1)}, f32[8,4,512,128]{3,2,1,0:T(8,128)S(1)}, bf16[3,8,2048]{2,1,0:T(8,128)(2,1)S(1)}, bf16[3,8,512]{2,1,0:T(8,128)(2,1)S(1)}, bf16[3,8,512]{2,1,0:T(8,128)(2,1)S(1)}) custom-call(bf16[8,2048]{1,0:T(8,128)(2,1)} %tokens.1, f32[1,2048]{1,0:T(1,128)} %bitcast.30, f32[1,32]{1,0:T(1,128)} %bitcast.33, ...), custom_call_target="tpu_custom_call" | custom-call | tf_op jit(solution)/shard_map/pallas_call | solution.py:390
  61.1 3.4 %shard_map.309 = (f32[8,4,512,128]{3,2,1,0:T(8,128)}, bf16[8,2048]{1,0:T(8,128)(2,1)}, bf16[3,8,2048]{2,1,0:T(8,128)(2,1)}, bf16[3,8,512]{2,1,0:T(8,128)(2,1)}, bf16[3,8,512]{2,1,0:T(8,128)(2,1)}) custom-call(f32[8,4,512,128]{3,2,1,0:T(8,128)S(1)} %get-tuple-element.15.refs_0_, bf16[8,2048]{1,0:T(8,128)(2,1)S(1)} %get-tuple-element.16.refs_1_, ...), custom_call_target="tpu_custom_call" | custom-call | tf_op jit(solution)/shard_map/pallas_call | solution.py:439

commit v2 on v1

--- a/solution.py
+++ b/solution.py
@@ -65,64 +65,105 @@
 MESH = pl.DeviceIdType.MESH
 BF16 = jnp.bfloat16
 F32 = jnp.float32
-
-
-def signal_all(n):
+EARLY = 1
+BEFORE = 4
+SMALL = range(16)
+
+
+def level(n):
+    side = 1
+    while side * side < n:
+        side += 1
+    return side
+
+
+def line_peer(k, side):
+    me = lax.axis_index("ep")
+    place, spot = me // side, me % side
+    upper = (2 * place) // side
+    place = place + upper * (side - 1 - 2 * place)
+    pick = k + (k - place + side) // side
+    return (pick + upper * (side - 1 - 2 * pick)) * side + spot
+
+
+def flip(spot, j):
+    bit = 1
+    while bit <= j:
+        if j & bit:
+            spot = spot + bit * (1 - 2 * ((spot // bit) % 2))
+        bit *= 2
+    return spot
+
+
+def plane_peer(j, side, block=None):
+    me = lax.axis_index("ep")
+    base = me if block is None else block
+    return (base // side) * side + flip(me % side, j)
+
+
+def remote(source, target, send_sem, recv_sem, p, t):
+    return pltpu.make_async_remote_copy(
+        source, target, send_sem, recv_sem,
+        device_id={"ep": p, "tp": t}, device_id_type=MESH,
+    )
+
+
+def signal_near(n):
     me, t = lax.axis_index("ep"), lax.axis_index("tp")
+    side = level(n)
     barrier = pltpu.get_barrier_semaphore()
-
-    def tell(off, carry):
-        p = lax.rem(me + off, n)
-        pl.semaphore_signal(barrier, inc=1, device_id={"ep": p, "tp": t}, device_id_type=MESH)
-        pl.semaphore_signal(barrier, inc=1, device_id={"ep": p, "tp": 1 - t}, device_id_type=MESH)
-        return carry
-
-    lax.fori_loop(1, n, tell, 0)
+    for k in range(side - 1):
+        for p in (line_peer(k, side), plane_peer(k + 1, side)):
+            pl.semaphore_signal(barrier, inc=1, device_id={"ep": p, "tp": t}, device_id_type=MESH)
     pl.semaphore_signal(barrier, inc=1, device_id={"ep": me, "tp": 1 - t}, device_id_type=MESH)
 
 
-def wait_all(n):
-    pl.semaphore_wait(pltpu.get_barrier_semaphore(), 2 * n - 1)
-
-
-def ep_send(n, source, target, send_sem, recv_sem):
+def wait_near(n):
+    pl.semaphore_wait(pltpu.get_barrier_semaphore(), 2 * (level(n) - 1) + 1)
+
+
+def bulk(ref, count, send_sem, recv_sem):
+    return partner_copy(ref.at[pl.ds(0, count)], ref.at[pl.ds(0, count)], send_sem, recv_sem)
+
+
+def gather_start(n, ref, send_sem, line_sem, plane_sem):
     me, t = lax.axis_index("ep"), lax.axis_index("tp")
-
-    def start(off, carry):
-        p = lax.rem(me + off, n)
-        pltpu.make_async_remote_copy(
-            source(p), target(me), send_sem.at[off], recv_sem.at[me],
-            device_id={"ep": p, "tp": t}, device_id_type=MESH,
+    side = level(n)
+    for k in range(side - 1):
+        remote(
+            ref.at[me], ref.at[me], send_sem, line_sem.at[me // side], line_peer(k, side), t
         ).start()
-        return carry
-
-    lax.fori_loop(1, n, start, 0)
-
-
-def ep_wait(n, target, send_sem, recv_sem, sends):
+    for j in reversed(range(1, side)):
+        remote(ref.at[me], ref.at[me], send_sem, plane_sem(me), plane_peer(j, side), t).start()
+
+
+def gather_forward(n, k, ref, send_sem, line_sem, plane_sem):
+    t = lax.axis_index("tp")
+    side = level(n)
+    block = line_peer(k, side)
+    bulk(ref, 1, send_sem, line_sem.at[block // side]).wait_recv()
+    for j in reversed(range(1, side)):
+        remote(
+            ref.at[block], ref.at[block], send_sem, plane_sem(block), plane_peer(j, side), t
+        ).start()
+
+
+def ep_send(n, source, target, send_sem, recv_sem, also=None):
     me, t = lax.axis_index("ep"), lax.axis_index("tp")
-
-    def finish(off, carry):
-        p = lax.rem(me + n - off, n)
-        copy = pltpu.make_async_remote_copy(
-            target(p), target(p), send_sem.at[off], recv_sem.at[p],
-            device_id={"ep": p, "tp": t}, device_id_type=MESH,
-        )
-        if sends:
-            copy.wait_send()
-        else:
-            copy.wait_recv()
-        return carry
-
-    lax.fori_loop(1, n, finish, 0)
+    side = level(n)
+    peers = [
+        plane_peer(j, side, line_peer(k, side))
+        for k in reversed(range(side - 1)) for j in reversed(range(side))
+    ] + [plane_peer(j, side) for j in reversed(range(1, side))]
+    for p in peers:
+        remote(source(p), target(me), send_sem, recv_sem, p, t).start()
+        if also is not None:
+            remote(source(p), target(me), *also, p, 1 - t).start()
 
 
 def partner_copy(source, target, send_sem, recv_sem):
     me, t = lax.axis_index("ep"), lax.axis_index("tp")
-    return pltpu.make_async_remote_copy(
-        source, target, send_sem, recv_sem,
-        device_id={"ep": me, "tp": 1 - t}, device_id_type=MESH,
-    )
+    return remote(source, target, send_sem, recv_sem, me, 1 - t)
 
 
 def short_conv_in(past, fresh, taps, window):
@@ -135,42 +176,70 @@
 
 
 def step_kernel(
-    n, capacity,
-    tokens, gain, step_bias, decay_rate, extra_decay, v_taps, i_taps, o_taps,
-    v_past, i_past, o_past, skip, group_gain, gain2, routes, route_weight,
-    state, gate_w, value_w, in_w, out_w, step_w, mix_w, cg_w, cu_w, cd_w, rg_w, ru_w, rd_w,
-    result, held, v_next, i_next, o_next,
-    mine, other, proj, back, old_mix, decays, columns,
-    gath, part, got, out_blk, arr, ret, home, share, theirs,
-    gw, vw, iw, ow, sw, wm, cg, cu, cd, rg, ru, rd,
-    wsem, ssem, gs, gr, ds0, dr0, rs, rr,
-    as_, ar, ps, pr, xs, xr, ds, dr, es, er, fs, fr, hs, hr,
+    n, capacity, *refs,
 ):
+    count = len(SMALL)
+    sources, refs = refs[:count], refs[count:]
+    state, *refs = refs
+    weight_refs, refs = refs[:12], refs[12:]
+    (result, held, v_next, i_next, o_next), refs = refs[:5], refs[5:]
+    smalls, refs = refs[:count], refs[count:]
+    (
+        tokens, gain, step_bias, decay_rate, extra_decay, v_taps, i_taps, o_taps,
+        v_past, i_past, o_past, skip, group_gain, gain2, routes, route_weight,
+    ) = smalls
+    (
+        mine, other, proj, back, old_mix, decays, columns,
+        gath, part, got, out_blk, arr, arr2, lend, borrow, ret, home,
+        share, theirs, half_out, half_in,
+    ), refs = refs[:21], refs[21:]
+    weight_bufs, refs = refs[:12], refs[12:]
+    gw, vw, iw, ow, sw, wm, cg, cu, cd, rg, ru, rd = weight_bufs
+    (
+        wsem, lsem, ssem, gs, gr, gp, ds0, dr0, rs, rr,
+        as_, ar, ap, ps, pr, xs, xr, es, er, cs, cr, ks, kr, fs, fr, hs, hr, ls, lr,
+    ) = refs
     me, t = lax.axis_index("ep"), lax.axis_index("tp")
-    signal_all(n)
+    side = level(n)
+    signal_near(n)
     rows, width = tokens.shape
     half = width // 2
-    piece = gate_w.shape[1]
+    quarter = half // 2
+    piece = gw.shape[1]
     groups, span, states = held.shape[1:]
     inner = groups * span
     heads = step_bias.shape[1]
     per_group = heads // groups
     head = span // per_group
-    pairs = (
-        (gate_w, gw), (value_w, vw), (in_w, iw), (out_w, ow), (step_w, sw), (mix_w, wm),
-        (cg_w, cg), (cu_w, cu), (rg_w, rg), (ru_w, ru), (rd_w, rd), (cd_w, cd),
-    )
-    loads = [pltpu.make_async_copy(x, y, wsem.at[i]) for i, (x, y) in enumerate(pairs)]
-    reads = [pltpu.make_async_copy(state.at[r], held.at[r], ssem.at[r]) for r in range(rows)]
-    for load in loads[:5] + reads + loads[5:]:
+    order = (2, 3, 4, 0, 1, 5, 6, 7, 9, 10, 8, 11)
+    fetch = [
+        pltpu.make_async_copy(x, y, lsem.at[i]) for i, (x, y) in enumerate(zip(sources, smalls))
+    ]
+    loads = [
+        pltpu.make_async_copy(x, y, wsem.at[i])
+        for i, (x, y) in enumerate(zip(weight_refs, weight_bufs))
+    ]
+    reads = [pltpu.make_async_copy(state, held, ssem)]
+    for load in fetch + [loads[i] for i in order[:3]]:
         load.start()
+    for load in fetch[:2]:
+        load.wait()
     normed = rms_scale(tokens[...], gain[...]).astype(BF16)
-    mine[me] = jnp.where(t == 0, normed[:, :half], normed[:, half:])
-    wait_all(n)
-    ep_send(n, lambda p: mine.at[me], lambda p: mine.at[p], gs, gr)
-
-    for load in loads[:5]:
+    halves = (normed[:, :half], normed[:, half:])
+    mine[me] = jnp.where(t == 0, halves[0], halves[1])
+    wait_near(n)
+
+    def own_plane(block):
+        return gp.at[block // side]
+
+    gather_start(n, mine, gs, gr, own_plane)
+    for load in [loads[i] for i in order[3:5]] + reads:
+        load.start()
+
+    for load in fetch[2:]:
         load.wait()
+    for i in (2, 3, 4):
+        loads[i].wait()
     in_rows = jnp.dot(normed, iw[...], preferred_element_type=F32).astype(BF16)
     out_rows = jnp.dot(normed, ow[...], preferred_element_type=F32).astype(BF16)
     step_raw = lax.dot_general(
@@ -212,9 +281,43 @@
         [jnp.where(low_lane, weighted, 0.0), jnp.where(low_lane, 0.0, weighted)], axis=0
     )
 
-    ep_wait(n, lambda p: mine.at[p], gs, gr, False)
-    cross = partner_copy(mine, other, ds0, dr0)
-    cross.start()
+
+    def pass_on(block, count):
+        bulk(mine, count, gs, own_plane(block)).wait_recv()
+        plane = pl.ds(pl.multiple_of((block // side) * side, side), side)
+        partner_copy(mine.at[plane], other.at[plane], ds0, dr0).start()
+
+    for k in range(side - 1):
+        gather_forward(n, k, mine, gs, gr, own_plane)
+    pass_on(me, side - 1)
+
+    span_row = lax.broadcasted_iota(jnp.int32, (rows, span), 0)
+
+    def read_state(g):
+        maps = out_conv[:, g * states : (g + 1) * states].astype(BF16)
+
+        def reduce_row(r, acc):
+            block = held[r, g].astype(BF16)
+            sums = lax.dot_general(
+                maps, block, (((1,), (1,)), ((), ())), preferred_element_type=F32
+            )
+            return jnp.where(span_row == r, sums, acc)
+
+        old_mix[:, g * span : (g + 1) * span] = lax.fori_loop(
+            0, rows, reduce_row, jnp.zeros((rows, span), F32)
+        )
+
+    for read in reads:
+        read.wait()
+    for i in order[5:]:
+        loads[i].start()
+    for g in range(EARLY):
+        read_state(g)
+    for k in range(side - 1):
+        pass_on(line_peer(k, side), side - 1)
+
+    for i in (0, 1):
+        loads[i].wait()
 
     def product(block_ref, start):
         block = block_ref[...].reshape(n * rows, half)
@@ -223,31 +326,18 @@
         ]
 
     first = product(mine, pl.multiple_of(t * half, half))
-    cross.wait_recv()
+
+    bulk(other, n, ds0, dr0).wait_recv()
     second = product(other, pl.multiple_of((1 - t) * half, half))
     for k in range(2):
         proj[:, k] = (first[k] + second[k]).astype(BF16).reshape(n, rows, piece)
     back[me] = proj[me]
     ep_send(n, lambda p: proj.at[p], lambda p: back.at[p], rs, rr)
 
-    for read in reads:
-        read.wait()
-    span_row = lax.broadcasted_iota(jnp.int32, (rows, span), 0)
-    for g in range(groups):
-        maps = out_conv[:, g * states : (g + 1) * states].astype(BF16)
-
-        def reduce_row(r, acc, g=g, maps=maps):
-            block = held[r, g].astype(BF16)
-            sums = lax.dot_general(
-                maps, block, (((1,), (1,)), ((), ())), preferred_element_type=F32
-            )
-            return jnp.where(span_row == r, sums, acc)
-
-        old_mix[:, g * span : (g + 1) * span] = lax.fori_loop(
-            0, rows, reduce_row, jnp.zeros((rows, span), F32)
-        )
-
-    ep_wait(n, lambda p: back.at[p], rs, rr, False)
+    for g in range(EARLY, groups):
+        read_state(g)
+
+    bulk(back, n - 1, rs, rr).wait_recv()
     gate_rows = jnp.concatenate([back[j, 0] for j in range(n)], axis=1).astype(F32)
     value_rows = jnp.concatenate([back[j, 1] for j in range(n)], axis=1)
     value_conv = short_conv_in(v_past, value_rows, v_taps, v_next)
@@ -263,7 +353,11 @@
         ) * gate[:, cut]
         mix = mix * lax.rsqrt(jnp.mean(mix * mix, axis=-1, keepdims=True) + EPSILON)
         gath[me, :, cut] = (mix * group_gain[:, cut]).astype(BF16)
-    ep_send(n, lambda p: gath.at[me], lambda p: gath.at[p], as_, ar)
+
+    def any_plane(block):
+        return ap
+
+    gather_start(n, gath, as_, ar, any_plane)
 
     top = scaled.astype(BF16).astype(F32)
     rest = scaled - top
@@ -286,91 +380,133 @@
                 held[r, g, at, :] = held[r, g, at, :] * factor + grown[at]
         return carry
 
-    lax.fori_loop(0, rows, update_row, 0)
-    for load in loads[5:]:
-        load.wait()
-    ep_wait(n, lambda p: gath.at[p], as_, ar, False)
+    lax.fori_loop(0, BEFORE, update_row, 0)
+    gather_forward(n, 0, gath, as_, ar, any_plane)
+    gather_forward(n, 1, gath, as_, ar, any_plane)
+    gather_forward(n, 2, gath, as_, ar, any_plane)
+    lax.fori_loop(BEFORE, rows, update_row, 0)
+    for i in range(5, 12):
+        loads[i].wait()
+    bulk(mine, n - 1, gs, gs).wait_send()
+    bulk(back, n - 1, rs, rr).wait_send()
+    bulk(other, n, ds0, dr0).wait_send()
+    bulk(gath, n - side, as_, ap).wait_recv()
     summed = jnp.dot(
         gath[...].reshape(n * rows, inner), wm[...], preferred_element_type=F32
     )
     part[...] = summed.astype(BF16).reshape(n, rows, piece)
     got[t, me] = part[me]
 
-    def start(off, carry):
-        p = lax.rem(me + off, n)
-        pltpu.make_async_remote_copy(
-            part.at[p], got.at[t, me], ps.at[off], pr.at[me],
-            device_id={"ep": p, "tp": t}, device_id_type=MESH,
-        ).start()
-        pltpu.make_async_remote_copy(
-            part.at[p], got.at[t, me], xs.at[off], xr.at[me],
-            device_id={"ep": p, "tp": 1 - t}, device_id_type=MESH,
-        ).start()
-        return carry
-
-    lax.fori_loop(1, n, start, 0)
-    near = partner_copy(part.at[me], got.at[t, me], ds, dr)
-    near.start()
-    near_in = partner_copy(part.at[me], got.at[1 - t, me], ds, dr)
-    near_in.wait_recv()
-    ep_wait(n, lambda p: got.at[t, p], ps, pr, False)
-    ep_wait(n, lambda p: got.at[1 - t, p], xs, xr, False)
+    partner_copy(part.at[me], got.at[t, me], xs, xr).start()
+    ep_send(n, lambda p: part.at[p], lambda p: got.at[t, p], ps, pr, (xs, xr))
+    bulk(gath, n - 1, as_, ap).wait_send()
+    same, cross = bulk(got.at[t], n - 1, ps, pr), bulk(got.at[1 - t], n, xs, xr)
+    same.wait_recv()
+    cross.wait_recv()
     both = (got[0].astype(F32) + got[1].astype(F32)).astype(BF16).astype(F32)
     mixed_out = jnp.concatenate([both[j] for j in range(n)], axis=1)
     stream = (tokens[...].astype(F32) + mixed_out).astype(BF16)
     ffn = rms_scale(stream, gain2[...]).astype(BF16)
 
+    def own_half(values):
+        return jnp.where(t == 0, values[:, :half], values[:, half:])
+
+    def far_half(values):
+        return jnp.where(t == 0, values[:, half:], values[:, :half])
+
     upper = lax.rem(lax.broadcasted_iota(jnp.int32, (n * rows, 1), 0), rows) >= rows // 2
-    left = jnp.dot(spread, ffn[:, :half], preferred_element_type=F32)
-    right = jnp.dot(spread, ffn[:, half:], preferred_element_type=F32)
-    out_blk[...] = jnp.where(upper, right, left).astype(BF16).reshape(n, rows, half)
+    ffn_own = own_half(ffn)
+    left = jnp.dot(spread, ffn_own[:, :quarter], preferred_element_type=F32)
+    right = jnp.dot(spread, ffn_own[:, quarter:], preferred_element_type=F32)
+    out_blk[...] = jnp.where(upper, right, left).astype(BF16).reshape(n, rows, quarter)
     arr[me] = out_blk[me]
-    ep_send(n, lambda p: out_blk.at[p], lambda p: arr.at[p], es, er)
+    ep_send(n, lambda p: out_blk.at[p], lambda p: arr.at[p], es, er.at[me // side])
     shared_hidden = (
         jax.nn.silu(jnp.dot(ffn, cg[...], preferred_element_type=F32))
         * jnp.dot(ffn, cu[...], preferred_element_type=F32)
     ).astype(BF16)
     shared = jnp.dot(shared_hidden, cd[...], preferred_element_type=F32)
-    ep_wait(n, lambda p: arr.at[p], es, er, False)
-
-    arrived = arr[...].reshape(n * rows, half)
-
-    def up(w):
-        low = jnp.dot(arrived, w[:half], preferred_element_type=F32)
-        high = jnp.dot(arrived, w[half:], preferred_element_type=F32)
+    share[...] = far_half(shared)
+    swap = partner_copy(share, theirs, hs, hr)
+    swap.start()
+    same.wait_send()
+    cross.wait_send()
+
+    def relay(block, count):
+        bulk(arr, count, es, er.at[block // side]).wait_recv()
+        plane = pl.ds(pl.multiple_of((block // side) * side, side), side)
+        partner_copy(arr.at[plane], arr2.at[plane], cs, cr).start()
+
+    relay(me, side - 1)
+    for k in range(side - 1):
+        relay(line_peer(k, side), side)
+
+    def part_dots(ref, w, start):
+        block = ref[...].reshape(n * rows, quarter)
+        return [
+            jnp.dot(
+                block, w[pl.ds(pl.multiple_of(start + k * quarter, quarter), quarter)],
+                preferred_element_type=F32,
+            )
+            for k in range(2)
+        ]
+
+    pre = [part_dots(arr, w, t * half) for w in (rg, ru)]
+
+    bulk(arr2, n, cs, cr).wait_recv()
+
+    def up(w, pair):
+        low, high = part_dots(arr2, w, (1 - t) * half)
+        low, high = low + pair[0], high + pair[1]
         count = n * rows
-        other = jnp.where(
+        swapped = jnp.where(
             upper, pltpu.roll(low, rows // 2, 0), pltpu.roll(high, count - rows // 2, 0)
         )
-        return jnp.where(upper, high, low) + other
-
-    hidden = (jax.nn.silu(up(rg)) * up(ru)).astype(BF16)
-    out_left = jnp.dot(hidden, rd[:, :half], preferred_element_type=F32)
-    out_right = jnp.dot(hidden, rd[:, half:], preferred_element_type=F32)
-    ret[...] = jnp.where(upper, out_right, out_left).astype(BF16).reshape(n, rows, half)
+        return jnp.where(upper, high, low) + swapped
+
+    hidden = (jax.nn.silu(up(rg, pre[0])) * up(ru, pre[1])).astype(BF16)
+
+    def down(start):
+        outs = [
+            jnp.dot(
+                hidden, rd[:, pl.ds(pl.multiple_of(start + k * quarter, quarter), quarter)],
+                preferred_element_type=F32,
+            )
+            for k in range(2)
+        ]
+        return jnp.where(upper, outs[1], outs[0])
+
+    lend[...] = down((1 - t) * half).astype(BF16).reshape(n, rows, quarter)
+    loan = partner_copy(lend, borrow, ks, kr)
+    loan.start()
+    own = down(t * half)
+    loan.wait_recv()
+    ret[...] = (own + borrow[...].reshape(n * rows, quarter).astype(F32)).astype(BF16).reshape(
+        n, rows, quarter
+    )
     home[me] = ret[me]
     ep_send(n, lambda p: ret.at[p], lambda p: home.at[p], fs, fr)
-    ep_wait(n, lambda p: home.at[p], fs, fr, False)
+    bulk(arr, n - 1, es, es).wait_send()
+    bulk(arr2, n, cs, cr).wait_send()
+    loan.wait_send()
+    swap.wait_send()
+    swap.wait_recv()
+    base = own_half(stream.astype(F32)) + (own_half(shared) + theirs[...])
+    bulk(home, n - 1, fs, fr).wait_recv()
     routed = jnp.dot(
-        combine, home[...].reshape(n * rows, half).astype(F32),
+        combine, home[...].reshape(n * rows, quarter).astype(F32),
         precision=lax.Precision.HIGHEST, preferred_element_type=F32,
     )
-    share[:, :half] = shared[:, :half] + routed[:rows]
-    share[:, half:] = shared[:, half:] + routed[rows:]
-    last = partner_copy(share, theirs, hs, hr)
+    routed = jnp.concatenate([routed[:rows], routed[rows:]], axis=1)
+    half_out[...] = (base + routed).astype(BF16)
+    last = partner_copy(half_out, half_in, ls, lr)
     last.start()
+    bulk(home, n - 1, fs, fr).wait_send()
     last.wait_recv()
-    result[...] = (stream.astype(F32) + (share[...] + theirs[...])).astype(BF16)
-    ep_wait(n, lambda p: gath.at[p], as_, ar, True)
-    ep_wait(n, lambda p: got.at[t, p], ps, pr, True)
-    ep_wait(n, lambda p: got.at[t, p], xs, xr, True)
-    near.wait_send()
-    ep_wait(n, lambda p: arr.at[p], es, er, True)
-    ep_wait(n, lambda p: home.at[p], fs, fr, True)
+    mine_half, far = half_out[...], half_in[...]
+    result[:, :half] = jnp.where(t == 0, mine_half, far)
+    result[:, half:] = jnp.where(t == 0, far, mine_half)
     last.wait_send()
-    ep_wait(n, lambda p: mine.at[p], gs, gr, True)
-    cross.wait_send()
-    ep_wait(n, lambda p: back.at[p], rs, rr, True)
 
 
 def mixer_step(n, capacity, small, state, weights):
@@ -381,11 +517,11 @@
     groups, span, _ = state.shape[1:]
     vmem, hbm = pl.BlockSpec(memory_space=pltpu.VMEM), pl.BlockSpec(memory_space=pl.ANY)
     dma = pltpu.SemaphoreType.DMA
-    many = dma((n,))
+    many = dma((level(n),))
     block = pltpu.VMEM((n, rows, half), BF16)
+    narrow = pltpu.VMEM((n, rows, half // 2), BF16)
     pieces = pltpu.VMEM((n, 2, rows, piece), BF16)
     heads = small[2].shape[1]
-    shape = jax.ShapeDtypeStruct
     mix_piece = weights[5].shape[1]
     return pl.pallas_call(
         functools.partial(step_kernel, n, capacity),
@@ -396,9 +532,10 @@
             pltpu.VMEM(small[9].shape, BF16),
             pltpu.VMEM(small[10].shape, BF16),
         ),
-        in_specs=[vmem] * len(small) + [hbm] * (1 + len(weights)),
+        in_specs=[hbm] * (len(small) + 1 + len(weights)),
         out_specs=(vmem,) * 5,
-        scratch_shapes=[
+        scratch_shapes=[pltpu.VMEM(a.shape, a.dtype) for a in small]
+        + [
             block, block, pieces, pieces,
             pltpu.VMEM((rows, inner), F32),
             pltpu.VMEM((rows, heads), F32),
@@ -406,18 +543,19 @@
             pltpu.VMEM((n, rows, inner), BF16),
             pltpu.VMEM((n, rows, mix_piece), BF16),
             pltpu.VMEM((2, n, rows, mix_piece), BF16),
-            block, block, block, block,
-            pltpu.VMEM((rows, width), F32),
-            pltpu.VMEM((rows, width), F32),
+            narrow, narrow, narrow, narrow, narrow, narrow, narrow,
+            pltpu.VMEM((rows, half), F32),
+            pltpu.VMEM((rows, half), F32),
+            pltpu.VMEM((rows, half), BF16),
+            pltpu.VMEM((rows, half), BF16),
         ]
-        + [pltpu.VMEM(w.shape, BF16) for w in weights[:9]]
-        + [pltpu.VMEM(w.shape, BF16) for w in weights[9:]]
-        + [dma((12,)), dma((rows,)), many, many, dma, dma, many, many]
-        + [many] * 6 + [dma, dma] + [many] * 4 + [dma, dma],
+        + [pltpu.VMEM(w.shape, BF16) for w in weights]
+        + [dma((len(weights),)), dma((len(small),)), dma, dma, many, many]
+        + [dma] * 5 + [many] + [dma] * 6 + [many] + [dma] * 10,
         compiler_params=pltpu.CompilerParams(
             collective_id=0, has_side_effects=True, vmem_limit_bytes=54 << 20
         ),
-    )(*small, state, *weights)
+    )(*[pltpu.with_memory_space_constraint(a, pltpu.HBM) for a in (*small, state, *weights)])
 
 
 def store_kernel(count, *refs):
@@ -524,7 +662,7 @@
     if tp != 2 or routed_w.shape[0] != 1 or rows != 8:
         return False
     capacity = (rows * routes.shape[1] + n - 1) // n + 1
-    return gate_w.shape[2] % 128 == 0 and mix_w.shape[1] % 128 == 0 and 2 * capacity == rows
+    return level(n) ** 2 == n and gate_w.shape[2] % 128 == 0 and mix_w.shape[1] % 128 == 0 and 2 * capacity == rows
 
 
 def shards(

time: 65.1 us -> 51.6 us (0.79)
  Pallas kernels: 63.9 us -> 50.8 us
    pallas_call x1, Pallas kernels: 60.5 us -> 47.4 us  [mixer_step(): pl.pallas_call(functools.partial(step_kernel, n, capacity), out_shape=(pl...]
where the time goes in v2:
time: 51.6 us; the launch traced here: 51.4 us
  Pallas kernels  50.8 us (98%)
  between operations  0.65 us (1%)
    pallas_call x1, Pallas kernels, mixer_step(): pl.pallas_call(functools.partial(step_kernel, n, capacity), out_shape=(pl...  47.4 us
    pallas_call x1, Pallas kernels, store(): pl.pallas_call(functools.partial(store_kernel, count), out_shape=tuple((j...  3.41 us

profile of v2, /device:TPU:0, one launch (start us, length us, event | category | flops | bytes accessed | tf_op | source)
XLA Modules:
  0.0 51.4 jit_solution(8606910995685857545)
XLA Ops:
  0.6 47.4 %shard_map.308 = (bf16[8,2048]{1,0:T(8,128)(2,1)S(1)}, f32[8,4,512,128]{3,2,1,0:T(8,128)S(1)}, bf16[3,8,2048]{2,1,0:T(8,128)(2,1)S(1)}, bf16[3,8,512]{2,1,0:T(8,128)(2,1)S(1)}, bf16[3,8,512]{2,1,0:T(8,128)(2,1)S(1)}) custom-call(bf16[8,2048]{1,0:T(8,128)(2,1)} %refs_0_.1, f32[1,2048]{1,0:T(1,128)} %bitcast.30, f32[1,32]{1,0:T(1,128)} %bitcast.33, ...), custom_call_target="tpu_custom_call" | custom-call | tf_op jit(solution)/shard_map/pallas_call | solution.py:526
  48.0 3.4 %shard_map.309 = (f32[8,4,512,128]{3,2,1,0:T(8,128)}, bf16[8,2048]{1,0:T(8,128)(2,1)}, bf16[3,8,2048]{2,1,0:T(8,128)(2,1)}, bf16[3,8,512]{2,1,0:T(8,128)(2,1)}, bf16[3,8,512]{2,1,0:T(8,128)(2,1)}) custom-call(f32[8,4,512,128]{3,2,1,0:T(8,128)S(1)} %get-tuple-element.15.refs_0_, bf16[8,2048]{1,0:T(8,128)(2,1)S(1)} %get-tuple-element.16.refs_1_, ...), custom_call_target="tpu_custom_call" | custom-call | tf_op jit(solution)/shard_map/pallas_call | solution.py:577

commit v3 on v2

--- a/solution.py
+++ b/solution.py
@@ -68,6 +68,7 @@
 EARLY = 1
 BEFORE = 4
 SMALL = range(16)
+TWIN = (0, 1, 5, 9, 10, 11)
 
 
 def level(n):
@@ -114,12 +115,15 @@
     barrier = pltpu.get_barrier_semaphore()
     for k in range(side - 1):
         for p in (line_peer(k, side), plane_peer(k + 1, side)):
-            pl.semaphore_signal(barrier, inc=1, device_id={"ep": p, "tp": t}, device_id_type=MESH)
+            for core in range(2):
+                pl.semaphore_signal(
+                    barrier, inc=1, device_id={"ep": p, "tp": core}, device_id_type=MESH
+                )
     pl.semaphore_signal(barrier, inc=1, device_id={"ep": me, "tp": 1 - t}, device_id_type=MESH)
 
 
 def wait_near(n):
-    pl.semaphore_wait(pltpu.get_barrier_semaphore(), 2 * (level(n) - 1) + 1)
+    pl.semaphore_wait(pltpu.get_barrier_semaphore(), 4 * (level(n) - 1) + 1)
 
 
 def bulk(ref, count, send_sem, recv_sem):
@@ -148,17 +152,121 @@
         ).start()
 
 
-def ep_send(n, source, target, send_sem, recv_sem, also=None):
+def home_core(n, p):
+    side = level(n)
+    return (p % side) // (side // 2)
+
+
+def home_spot(n, p):
+    side = level(n)
+    return (p // side) * (side // 2) + p % (side // 2)
+
+
+def at_spot(n, i):
+    side = level(n)
+    half_side = side // 2
+    return (i // half_side) * side + lax.axis_index("tp") * half_side + i % half_side
+
+
+def is_home(n):
+    return lax.axis_index("tp") == home_core(n, lax.axis_index("ep"))
+
+
+def by_home(n, at_home, away):
+    home = is_home(n)
+
+    @pl.when(home)
+    def _():
+        at_home()
+
+    @pl.when(jnp.logical_not(home))
+    def _():
+        away()
+
+
+def rows_start(n, stage, rows_ref, send_sem, line_sem, plane_sem):
     me, t = lax.axis_index("ep"), lax.axis_index("tp")
     side = level(n)
-    peers = [
-        plane_peer(j, side, line_peer(k, side))
-        for k in reversed(range(side - 1)) for j in reversed(range(side))
-    ] + [plane_peer(j, side) for j in reversed(range(1, side))]
-    for p in peers:
-        remote(source(p), target(me), send_sem, recv_sem, p, t).start()
-        if also is not None:
-            remote(source(p), target(me), *also, p, 1 - t).start()
+    core = home_core(n, me)
+    target = rows_ref.at[t, home_spot(n, me)]
+    arrive = line_sem.at[(me // side) * 2 + t]
+    for k in range(side - 1):
+        remote(stage, target, send_sem, arrive, line_peer(k, side), core).start()
+    for j in reversed(range(1, side)):
+        remote(stage, target, send_sem, plane_sem, plane_peer(j, side), core).start()
+
+
+def rows_forward(n, k, rows_ref, send_sem, line_sem, plane_sem):
+    t = lax.axis_index("tp")
+    side = level(n)
+
+    @pl.when(is_home(n))
+    def _():
+        q = line_peer(k, side)
+        for f in range(2):
+            block = rows_ref.at[f, home_spot(n, q)]
+            arrive = line_sem.at[(q // side) * 2 + f]
+            partner_copy(block, block, send_sem.at[k], arrive).wait_recv()
+            for j in reversed(range(1, side)):
+                remote(block, block, send_sem.at[k], plane_sem, plane_peer(j, side), t).start()
+
+
+def rows_wait(n, rows_ref, send_sem, plane_sem):
+    def arrived(count):
+        block = rows_ref.at[:, pl.ds(0, count)]
+        partner_copy(block, block, send_sem, plane_sem).wait_recv()
+
+    hn = n // 2
+    by_home(n, lambda: arrived(hn - level(n)), lambda: arrived(hn))
+
+
+def rows_sent(n, rows_ref, own_sem, send_sem):
+    side = level(n)
+    bulk(rows_ref.at[0], 2 * (side - 1), own_sem, own_sem).wait_send()
+
+    @pl.when(is_home(n))
+    def _():
+        block = rows_ref.at[:, pl.ds(0, side - 1)]
+        for k in range(side - 1):
+            partner_copy(block, block, send_sem.at[k], send_sem.at[k]).wait_send()
+
+
+def back_start(n, source, target, send_sem, recv_sem):
+    me, t = lax.axis_index("ep"), lax.axis_index("tp")
+    hn = n // 2
+    for j in reversed(range(1, hn)):
+        i = flip(home_spot(n, me), j)
+        for core in range(2):
+            remote(
+                source.at[core, i], target.at[me], send_sem, recv_sem, at_spot(n, i), core
+            ).start()
+    i = home_spot(n, me)
+
+    def at_home():
+        partner_copy(source.at[1 - t, i], target.at[me], send_sem, recv_sem).start()
+        target[me] = source[t, i]
+
+    def away():
+        for core in range(2):
+            remote(
+                source.at[core, i], target.at[me], send_sem, recv_sem, at_spot(n, i), core
+            ).start()
+
+    by_home(n, at_home, away)
+
+
+def back_wait(n, target, send_sem, recv_sem):
+    by_home(
+        n, lambda: bulk(target, n - 1, send_sem, recv_sem).wait_recv(),
+        lambda: bulk(target, n, send_sem, recv_sem).wait_recv(),
+    )
+
+
+def back_sent(n, target, send_sem, recv_sem):
+    by_home(
+        n, lambda: bulk(target, n - 1, send_sem, recv_sem).wait_send(),
+        lambda: bulk(target, n, send_sem, recv_sem).wait_send(),
+    )
 
 
 def partner_copy(source, target, send_sem, recv_sem):
@@ -189,15 +297,15 @@
         v_past, i_past, o_past, skip, group_gain, gain2, routes, route_weight,
     ) = smalls
     (
-        mine, other, proj, back, old_mix, decays, columns,
-        gath, part, got, out_blk, arr, arr2, lend, borrow, ret, home,
+        stage, row_buf, proj, back, old_mix, decays, columns,
+        mixed, gath, early_out, early_in, blocks, sx, own_rows, ret, home,
         share, theirs, half_out, half_in,
-    ), refs = refs[:21], refs[21:]
+    ), refs = refs[:20], refs[20:]
     weight_bufs, refs = refs[:12], refs[12:]
     gw, vw, iw, ow, sw, wm, cg, cu, cd, rg, ru, rd = weight_bufs
     (
-        wsem, lsem, ssem, gs, gr, gp, ds0, dr0, rs, rr,
-        as_, ar, ap, ps, pr, xs, xr, es, er, cs, cr, ks, kr, fs, fr, hs, hr, ls, lr,
+        wsem, lsem, ssem, ts, tr, gs, gf, gl, gp, rs, rr, es, er,
+        as_, af, al, ap, ns, nr, ps, pr, pp, fs, fr, os_, or_, hs, hr, ls, lr,
     ) = refs
     me, t = lax.axis_index("ep"), lax.axis_index("tp")
     side = level(n)
@@ -205,7 +313,10 @@
     rows, width = tokens.shape
     half = width // 2
     quarter = half // 2
-    piece = gw.shape[1]
+    piece = gw.shape[2]
+    hn = n // 2
+    spot = home_spot(n, me)
+    at_home = is_home(n)
     groups, span, states = held.shape[1:]
     inner = groups * span
     heads = step_bias.shape[1]
@@ -216,8 +327,12 @@
         pltpu.make_async_copy(x, y, lsem.at[i]) for i, (x, y) in enumerate(zip(sources, smalls))
     ]
     loads = [
-        pltpu.make_async_copy(x, y, wsem.at[i])
+        pltpu.make_async_copy(x, y.at[t] if i in TWIN else y, wsem.at[i])
         for i, (x, y) in enumerate(zip(weight_refs, weight_bufs))
+    ]
+    twins = [
+        partner_copy(weight_refs[i], weight_bufs[i].at[t], ts.at[k], tr.at[k])
+        for k, i in enumerate(TWIN)
     ]
     reads = [pltpu.make_async_copy(state, held, ssem)]
     for load in fetch + [loads[i] for i in order[:3]]:
@@ -225,14 +340,24 @@
     for load in fetch[:2]:
         load.wait()
     normed = rms_scale(tokens[...], gain[...]).astype(BF16)
-    halves = (normed[:, :half], normed[:, half:])
-    mine[me] = jnp.where(t == 0, halves[0], halves[1])
+
+    def own_half(values):
+        return jnp.where(t == 0, values[:, :half], values[:, half:])
+
+    def far_half(values):
+        return jnp.where(t == 0, values[:, half:], values[:, :half])
+
+    stage[...] = own_half(normed)
+
+    @pl.when(at_home)
+    def _():
+        row_buf[0, spot] = normed[:, :half]
+        row_buf[1, spot] = normed[:, half:]
+
     wait_near(n)
-
-    def own_plane(block):
-        return gp.at[block // side]
-
-    gather_start(n, mine, gs, gr, own_plane)
+    rows_start(n, stage, row_buf, gs, gl, gp)
+    for twin in twins[:2]:
+        twin.start()
     for load in [loads[i] for i in order[3:5]] + reads:
         load.start()
 
@@ -281,15 +406,22 @@
         [jnp.where(low_lane, weighted, 0.0), jnp.where(low_lane, 0.0, weighted)], axis=0
     )
 
-
-    def pass_on(block, count):
-        bulk(mine, count, gs, own_plane(block)).wait_recv()
-        plane = pl.ds(pl.multiple_of((block // side) * side, side), side)
-        partner_copy(mine.at[plane], other.at[plane], ds0, dr0).start()
+    place = jnp.where(
+        lax.broadcasted_iota(jnp.int32, (rows, piece), 1)
+        == lax.broadcasted_iota(jnp.int32, (rows, piece), 0) + spot * rows,
+        1.0, 0.0,
+    ).astype(BF16)
+    picks = jnp.dot(spread, place, preferred_element_type=F32).astype(BF16)
+    early_out[:, 1] = picks.reshape(n, rows, piece)
+    for c in range(n):
+        early_out[c, 0] = tokens[:, c * piece : (c + 1) * piece]
+
+    @pl.when(at_home)
+    def _():
+        early_in[spot] = early_out[me]
 
     for k in range(side - 1):
-        gather_forward(n, k, mine, gs, gr, own_plane)
-    pass_on(me, side - 1)
+        rows_forward(n, k, row_buf, gf, gl, gp)
 
     span_row = lax.broadcasted_iota(jnp.int32, (rows, span), 0)
 
@@ -311,33 +443,41 @@
         read.wait()
     for i in order[5:]:
         loads[i].start()
+    for twin in twins[2:]:
+        twin.start()
     for g in range(EARLY):
         read_state(g)
-    for k in range(side - 1):
-        pass_on(line_peer(k, side), side - 1)
-
+    rows_wait(n, row_buf, gs, gp)
     for i in (0, 1):
         loads[i].wait()
-
-    def product(block_ref, start):
-        block = block_ref[...].reshape(n * rows, half)
-        return [
-            jnp.dot(block, w[pl.ds(start, half)], preferred_element_type=F32) for w in (gw, vw)
-        ]
-
-    first = product(mine, pl.multiple_of(t * half, half))
-
-    bulk(other, n, ds0, dr0).wait_recv()
-    second = product(other, pl.multiple_of((1 - t) * half, half))
-    for k in range(2):
-        proj[:, k] = (first[k] + second[k]).astype(BF16).reshape(n, rows, piece)
-    back[me] = proj[me]
-    ep_send(n, lambda p: proj.at[p], lambda p: back.at[p], rs, rr)
+    for twin in twins[:2]:
+        twin.wait_recv()
+    arrived = [row_buf[f].reshape(hn * rows, half) for f in range(2)]
+    for core in range(2):
+        for k, w in enumerate((gw, vw)):
+            made = sum(
+                jnp.dot(
+                    arrived[f], w[core, f * half : (f + 1) * half], preferred_element_type=F32
+                )
+                for f in range(2)
+            )
+            proj[core, :, k] = made.astype(BF16).reshape(hn, rows, piece)
+    back_start(n, proj, back, rs, rr)
+
+    @pl.when(at_home)
+    def _():
+        for k in reversed(range(side - 1)):
+            for j in reversed(range(side)):
+                p = plane_peer(j, side, line_peer(k, side))
+                remote(early_out.at[p], early_in.at[spot], es, er, p, t).start()
+        for j in reversed(range(1, side)):
+            p = plane_peer(j, side)
+            remote(early_out.at[p], early_in.at[spot], es, er, p, t).start()
 
     for g in range(EARLY, groups):
         read_state(g)
 
-    bulk(back, n - 1, rs, rr).wait_recv()
+    back_wait(n, back, rs, rr)
     gate_rows = jnp.concatenate([back[j, 0] for j in range(n)], axis=1).astype(F32)
     value_rows = jnp.concatenate([back[j, 1] for j in range(n)], axis=1)
     value_conv = short_conv_in(v_past, value_rows, v_taps, v_next)
@@ -352,12 +492,15 @@
             + skip_wide[:, cut] * value_conv[:, cut]
         ) * gate[:, cut]
         mix = mix * lax.rsqrt(jnp.mean(mix * mix, axis=-1, keepdims=True) + EPSILON)
-        gath[me, :, cut] = (mix * group_gain[:, cut]).astype(BF16)
-
-    def any_plane(block):
-        return ap
-
-    gather_start(n, gath, as_, ar, any_plane)
+        mixed[:, cut] = (mix * group_gain[:, cut]).astype(BF16)
+
+    rows_start(n, mixed, gath, as_, al, ap)
+    hand = partner_copy(mixed, gath.at[t, spot], ns, nr)
+
+    def keep():
+        gath[t, spot] = mixed[...]
+
+    by_home(n, keep, hand.start)
 
     top = scaled.astype(BF16).astype(F32)
     rest = scaled - top
@@ -381,118 +524,94 @@
         return carry
 
     lax.fori_loop(0, BEFORE, update_row, 0)
-    gather_forward(n, 0, gath, as_, ar, any_plane)
-    gather_forward(n, 1, gath, as_, ar, any_plane)
-    gather_forward(n, 2, gath, as_, ar, any_plane)
+    rows_forward(n, 0, gath, af, al, ap)
+    rows_forward(n, 1, gath, af, al, ap)
+    rows_forward(n, 2, gath, af, al, ap)
     lax.fori_loop(BEFORE, rows, update_row, 0)
     for i in range(5, 12):
         loads[i].wait()
-    bulk(mine, n - 1, gs, gs).wait_send()
-    bulk(back, n - 1, rs, rr).wait_send()
-    bulk(other, n, ds0, dr0).wait_send()
-    bulk(gath, n - side, as_, ap).wait_recv()
-    summed = jnp.dot(
-        gath[...].reshape(n * rows, inner), wm[...], preferred_element_type=F32
-    )
-    part[...] = summed.astype(BF16).reshape(n, rows, piece)
-    got[t, me] = part[me]
-
-    partner_copy(part.at[me], got.at[t, me], xs, xr).start()
-    ep_send(n, lambda p: part.at[p], lambda p: got.at[t, p], ps, pr, (xs, xr))
-    bulk(gath, n - 1, as_, ap).wait_send()
-    same, cross = bulk(got.at[t], n - 1, ps, pr), bulk(got.at[1 - t], n, xs, xr)
-    same.wait_recv()
-    cross.wait_recv()
-    both = (got[0].astype(F32) + got[1].astype(F32)).astype(BF16).astype(F32)
-    mixed_out = jnp.concatenate([both[j] for j in range(n)], axis=1)
-    stream = (tokens[...].astype(F32) + mixed_out).astype(BF16)
+    for twin in twins:
+        twin.wait_send()
+    for twin in twins[2:]:
+        twin.wait_recv()
+    rows_sent(n, row_buf, gs, gf)
+    back_sent(n, back, rs, rr)
+    by_home(
+        n, lambda: bulk(early_in, hn - 1, es, er).wait_recv(),
+        lambda: bulk(early_in, hn, es, er).wait_recv(),
+    )
+
+    @pl.when(at_home)
+    def _():
+        bulk(early_out, n - 1, es, er).wait_send()
+
+    by_home(n, partner_copy(mixed, gath.at[1 - t, spot], ns, nr).wait_recv, hand.wait_send)
+    rows_wait(n, gath, as_, ap)
+    both = sum(
+        jnp.dot(
+            gath[f].reshape(hn * rows, inner), wm[f], preferred_element_type=F32
+        ).astype(BF16).astype(F32)
+        for f in range(2)
+    ).astype(BF16).astype(F32)
+    block = early_in[:, 0].reshape(hn * rows, piece).astype(F32)
+    blocks[me] = (block + both).astype(BF16)
+
+    def any_plane(block):
+        return pp
+
+    gather_start(n, blocks, ps, pr, any_plane)
+    rows_sent(n, gath, as_, af)
+    for k in range(side - 1):
+        gather_forward(n, k, blocks, ps, pr, any_plane)
+    bulk(blocks, n - side, ps, pp).wait_recv()
+    stream = jnp.concatenate([blocks[j] for j in range(n)], axis=1)
+    sx[...] = stream.reshape(hn, rows, width)
+    give = partner_copy(sx.at[spot], own_rows, os_, or_)
+
+    @pl.when(at_home)
+    def _():
+        own_rows[...] = sx[spot]
+        give.start()
+
     ffn = rms_scale(stream, gain2[...]).astype(BF16)
-
-    def own_half(values):
-        return jnp.where(t == 0, values[:, :half], values[:, half:])
-
-    def far_half(values):
-        return jnp.where(t == 0, values[:, half:], values[:, :half])
-
-    upper = lax.rem(lax.broadcasted_iota(jnp.int32, (n * rows, 1), 0), rows) >= rows // 2
-    ffn_own = own_half(ffn)
-    left = jnp.dot(spread, ffn_own[:, :quarter], preferred_element_type=F32)
-    right = jnp.dot(spread, ffn_own[:, quarter:], preferred_element_type=F32)
-    out_blk[...] = jnp.where(upper, right, left).astype(BF16).reshape(n, rows, quarter)
-    arr[me] = out_blk[me]
-    ep_send(n, lambda p: out_blk.at[p], lambda p: arr.at[p], es, er.at[me // side])
+    upper = lax.rem(lax.broadcasted_iota(jnp.int32, (hn * rows, 1), 0), rows) >= rows // 2
+    pick = early_in[:, 1].reshape(hn * rows, piece)[:, : hn * rows]
+    hidden = []
+    for f in range(2):
+        unit = (
+            jax.nn.silu(jnp.dot(ffn, rg[f], preferred_element_type=F32))
+            * jnp.dot(ffn, ru[f], preferred_element_type=F32)
+        ).astype(BF16)
+        hidden.append(jnp.dot(pick, unit, preferred_element_type=F32).astype(BF16))
+    for core in range(2):
+        outs = [
+            sum(
+                jnp.dot(
+                    hidden[f], rd[f, :, q * quarter : (q + 1) * quarter],
+                    preferred_element_type=F32,
+                )
+                for f in range(2)
+            )
+            for q in (2 * core, 2 * core + 1)
+        ]
+        ret[core] = jnp.where(upper, outs[1], outs[0]).astype(BF16).reshape(hn, rows, quarter)
+    back_start(n, ret, home, fs, fr)
+    by_home(n, give.wait_send, give.wait_recv)
+    mine = own_rows[...]
+    mine_ffn = rms_scale(mine, gain2[...]).astype(BF16)
     shared_hidden = (
-        jax.nn.silu(jnp.dot(ffn, cg[...], preferred_element_type=F32))
-        * jnp.dot(ffn, cu[...], preferred_element_type=F32)
+        jax.nn.silu(jnp.dot(mine_ffn, cg[...], preferred_element_type=F32))
+        * jnp.dot(mine_ffn, cu[...], preferred_element_type=F32)
     ).astype(BF16)
     shared = jnp.dot(shared_hidden, cd[...], preferred_element_type=F32)
     share[...] = far_half(shared)
     swap = partner_copy(share, theirs, hs, hr)
     swap.start()
-    same.wait_send()
-    cross.wait_send()
-
-    def relay(block, count):
-        bulk(arr, count, es, er.at[block // side]).wait_recv()
-        plane = pl.ds(pl.multiple_of((block // side) * side, side), side)
-        partner_copy(arr.at[plane], arr2.at[plane], cs, cr).start()
-
-    relay(me, side - 1)
-    for k in range(side - 1):
-        relay(line_peer(k, side), side)
-
-    def part_dots(ref, w, start):
-        block = ref[...].reshape(n * rows, quarter)
-        return [
-            jnp.dot(
-                block, w[pl.ds(pl.multiple_of(start + k * quarter, quarter), quarter)],
-                preferred_element_type=F32,
-            )
-            for k in range(2)
-        ]
-
-    pre = [part_dots(arr, w, t * half) for w in (rg, ru)]
-
-    bulk(arr2, n, cs, cr).wait_recv()
-
-    def up(w, pair):
-        low, high = part_dots(arr2, w, (1 - t) * half)
-        low, high = low + pair[0], high + pair[1]
-        count = n * rows
-        swapped = jnp.where(
-            upper, pltpu.roll(low, rows // 2, 0), pltpu.roll(high, count - rows // 2, 0)
-        )
-        return jnp.where(upper, high, low) + swapped
-
-    hidden = (jax.nn.silu(up(rg, pre[0])) * up(ru, pre[1])).astype(BF16)
-
-    def down(start):
-        outs = [
-            jnp.dot(
-                hidden, rd[:, pl.ds(pl.multiple_of(start + k * quarter, quarter), quarter)],
-                preferred_element_type=F32,
-            )
-            for k in range(2)
-        ]
-        return jnp.where(upper, outs[1], outs[0])
-
-    lend[...] = down((1 - t) * half).astype(BF16).reshape(n, rows, quarter)
-    loan = partner_copy(lend, borrow, ks, kr)
-    loan.start()
-    own = down(t * half)
-    loan.wait_recv()
-    ret[...] = (own + borrow[...].reshape(n * rows, quarter).astype(F32)).astype(BF16).reshape(
-        n, rows, quarter
-    )
-    home[me] = ret[me]
-    ep_send(n, lambda p: ret.at[p], lambda p: home.at[p], fs, fr)
-    bulk(arr, n - 1, es, es).wait_send()
-    bulk(arr2, n, cs, cr).wait_send()
-    loan.wait_send()
+    bulk(blocks, n - 1, ps, pp).wait_send()
+    swap.wait_recv()
+    base = own_half(mine.astype(F32)) + (own_half(shared) + theirs[...])
     swap.wait_send()
-    swap.wait_recv()
-    base = own_half(stream.astype(F32)) + (own_half(shared) + theirs[...])
-    bulk(home, n - 1, fs, fr).wait_recv()
+    back_wait(n, home, fs, fr)
     routed = jnp.dot(
         combine, home[...].reshape(n * rows, quarter).astype(F32),
         precision=lax.Precision.HIGHEST, preferred_element_type=F32,
@@ -501,11 +620,11 @@
     half_out[...] = (base + routed).astype(BF16)
     last = partner_copy(half_out, half_in, ls, lr)
     last.start()
-    bulk(home, n - 1, fs, fr).wait_send()
+    back_sent(n, home, fs, fr)
     last.wait_recv()
-    mine_half, far = half_out[...], half_in[...]
-    result[:, :half] = jnp.where(t == 0, mine_half, far)
-    result[:, half:] = jnp.where(t == 0, far, mine_half)
+    near, far = half_out[...], half_in[...]
+    result[:, :half] = jnp.where(t == 0, near, far)
+    result[:, half:] = jnp.where(t == 0, far, near)
     last.wait_send()
 
 
@@ -517,12 +636,9 @@
     groups, span, _ = state.shape[1:]
     vmem, hbm = pl.BlockSpec(memory_space=pltpu.VMEM), pl.BlockSpec(memory_space=pl.ANY)
     dma = pltpu.SemaphoreType.DMA
-    many = dma((level(n),))
-    block = pltpu.VMEM((n, rows, half), BF16)
-    narrow = pltpu.VMEM((n, rows, half // 2), BF16)
-    pieces = pltpu.VMEM((n, 2, rows, piece), BF16)
+    many, twice = dma((level(n),)), dma((2 * level(n),))
+    hn = n // 2
     heads = small[2].shape[1]
-    mix_piece = weights[5].shape[1]
     return pl.pallas_call(
         functools.partial(step_kernel, n, capacity),
         out_shape=(
@@ -536,22 +652,34 @@
         out_specs=(vmem,) * 5,
         scratch_shapes=[pltpu.VMEM(a.shape, a.dtype) for a in small]
         + [
-            block, block, pieces, pieces,
+            pltpu.VMEM((rows, half), BF16),
+            pltpu.VMEM((2, hn, rows, half), BF16),
+            pltpu.VMEM((2, hn, 2, rows, piece), BF16),
+            pltpu.VMEM((n, 2, rows, piece), BF16),
             pltpu.VMEM((rows, inner), F32),
             pltpu.VMEM((rows, heads), F32),
             pltpu.VMEM((inner, 3 * rows), BF16),
-            pltpu.VMEM((n, rows, inner), BF16),
-            pltpu.VMEM((n, rows, mix_piece), BF16),
-            pltpu.VMEM((2, n, rows, mix_piece), BF16),
-            narrow, narrow, narrow, narrow, narrow, narrow, narrow,
+            pltpu.VMEM((rows, inner), BF16),
+            pltpu.VMEM((2, hn, rows, inner), BF16),
+            pltpu.VMEM((n, 2, rows, piece), BF16),
+            pltpu.VMEM((hn, 2, rows, piece), BF16),
+            pltpu.VMEM((n, hn * rows, piece), BF16),
+            pltpu.VMEM((hn, rows, width), BF16),
+            pltpu.VMEM((rows, width), BF16),
+            pltpu.VMEM((2, hn, rows, half // 2), BF16),
+            pltpu.VMEM((n, rows, half // 2), BF16),
             pltpu.VMEM((rows, half), F32),
             pltpu.VMEM((rows, half), F32),
             pltpu.VMEM((rows, half), BF16),
             pltpu.VMEM((rows, half), BF16),
         ]
-        + [pltpu.VMEM(w.shape, BF16) for w in weights]
-        + [dma((len(weights),)), dma((len(small),)), dma, dma, many, many]
-        + [dma] * 5 + [many] + [dma] * 6 + [many] + [dma] * 10,
+        + [
+            pltpu.VMEM((2, *w.shape) if i in TWIN else w.shape, BF16)
+            for i, w in enumerate(weights)
+        ]
+        + [dma((len(weights),)), dma((len(small),)), dma, dma((len(TWIN),)), dma((len(TWIN),))]
+        + [dma, many, twice, dma] + [dma] * 4 + [dma, many, twice, dma] + [dma] * 2
+        + [dma, many, dma] + [dma] * 8,
         compiler_params=pltpu.CompilerParams(
             collective_id=0, has_side_effects=True, vmem_limit_bytes=54 << 20
         ),
@@ -662,7 +790,7 @@
     if tp != 2 or routed_w.shape[0] != 1 or rows != 8:
         return False
     capacity = (rows * routes.shape[1] + n - 1) // n + 1
-    return level(n) ** 2 == n and gate_w.shape[2] % 128 == 0 and mix_w.shape[1] % 128 == 0 and 2 * capacity == rows
+    return level(n) ** 2 == n and n // 2 * rows <= mix_w.shape[1] == gate_w.shape[2] and gate_w.shape[2] % 128 == 0 and mix_w.shape[1] % 128 == 0 and 2 * capacity == rows
 
 
 def shards(

time: 51.6 us -> 48.1 us (0.932)
  Pallas kernels: 50.8 us -> 47.3 us
    pallas_call x1, Pallas kernels: 47.4 us -> 43.8 us  [mixer_step(): pl.pallas_call(functools.partial(step_kernel, n, capacity), out_shape=(pl...]
where the time goes in v3:
time: 48.1 us; the launch traced here: 47.9 us
  Pallas kernels  47.3 us (98%)
  between operations  0.65 us (1%)
    pallas_call x1, Pallas kernels, mixer_step(): pl.pallas_call(functools.partial(step_kernel, n, capacity), out_shape=(pl...  43.8 us
    pallas_call x1, Pallas kernels, store(): pl.pallas_call(functools.partial(store_kernel, count), out_shape=tuple((j...  3.41 us

profile of v3, /device:TPU:0, one launch (start us, length us, event | category | flops | bytes accessed | tf_op | source)
XLA Modules:
  0.0 47.9 jit_solution(17678527732043528472)
XLA Ops:
  0.6 43.8 %shard_map.308 = (bf16[8,2048]{1,0:T(8,128)(2,1)S(1)}, f32[8,4,512,128]{3,2,1,0:T(8,128)S(1)}, bf16[3,8,2048]{2,1,0:T(8,128)(2,1)S(1)}, bf16[3,8,512]{2,1,0:T(8,128)(2,1)S(1)}, bf16[3,8,512]{2,1,0:T(8,128)(2,1)S(1)}) custom-call(bf16[8,2048]{1,0:T(8,128)(2,1)} %refs_0_.1, f32[1,2048]{1,0:T(1,128)} %bitcast.30, f32[1,32]{1,0:T(1,128)} %bitcast.33, ...), custom_call_target="tpu_custom_call" | custom-call | tf_op jit(solution)/shard_map/pallas_call | solution.py:642
  44.5 3.4 %shard_map.309 = (f32[8,4,512,128]{3,2,1,0:T(8,128)}, bf16[8,2048]{1,0:T(8,128)(2,1)}, bf16[3,8,2048]{2,1,0:T(8,128)(2,1)}, bf16[3,8,512]{2,1,0:T(8,128)(2,1)}, bf16[3,8,512]{2,1,0:T(8,128)(2,1)}) custom-call(f32[8,4,512,128]{3,2,1,0:T(8,128)S(1)} %get-tuple-element.15.refs_0_, bf16[8,2048]{1,0:T(8,128)(2,1)S(1)} %get-tuple-element.16.refs_1_, ...), custom_call_target="tpu_custom_call" | custom-call | tf_op jit(solution)/shard_map/pallas_call | solution.py:705
